TPU v7x, 32 devices: a whole 2x2x4 slice. The times are simulated.
32 devices in a mesh: fs: 8 (over z, core), tp: 4 (over y, x).
Axes of the slice: x: 2, y: 2, z: 4, core: 2. Of those that a mesh axis runs over, the one named last changes fastest.
Arguments:
- in_saved: bfloat16 [6144, 2048], P(('fs', 'tp')), may hold values from -6 to 6
- in_cotangent: bfloat16 [6144, 2048], P(('fs', 'tp')), as said below
- point_saved: bfloat16 [6144, 2048], P(('fs', 'tp')), may hold values from -6 to 6
- point_cotangent: bfloat16 [6144, 2048], P(('fs', 'tp')), as said below
- in_basis: bfloat16 [2048, 128], replicated, as said below
- point_basis: bfloat16 [2048, 128], replicated, as said below
- in_first: float32 [128, 2048], P('fs', 'tp'), may hold values from -3 to 3
- in_second: float32 [128, 2048], P('fs', 'tp'), may hold values from 0.02 to 2
- point_first: float32 [128, 2048], P('fs', 'tp'), may hold values from -3 to 3
- point_second: float32 [128, 2048], P('fs', 'tp'), may hold values from 0.02 to 2
- in_master: float32 [2048, 2048], P('fs', 'tp'), may hold values from -3 to 3
- point_master: float32 [2048, 2048], P('fs', 'tp'), may hold values from -3 to 3
Outputs:
- in_first_new: float32 [128, 2048], P('fs', 'tp')
- in_second_new: float32 [128, 2048], P('fs', 'tp')
- point_first_new: float32 [128, 2048], P('fs', 'tp')
- point_second_new: float32 [128, 2048], P('fs', 'tp')
- in_step: float32 [2048, 2048], P('fs', 'tp')
- point_step: float32 [2048, 2048], P('fs', 'tp')
- in_master_new: float32 [2048, 2048], P('fs', 'tp')
- point_master_new: float32 [2048, 2048], P('fs', 'tp')
- in_copy: bfloat16 [2048, 2048], P(None, 'tp')
- point_copy: bfloat16 [2048, 2048], P(None, 'tp')
Inputs may be any that keep to these rules, and one draw needn't show every extreme that they name: `in_cotangent`: real-valued entries of every column. `point_cotangent`: real-valued entries of every column. `in_basis`: real-valued basis of full rank. `point_basis`: real-valued basis of full rank.
All inputs are finite; a program needn't handle non-finite values.
Results may differ from a plain program's by a relative error of at most 0.0034.
Values may be sent and summed in bfloat16 or wider, within the bound.
No kernel may reach another device: no remote copies, remote signals or barrier semaphores. Data moves between devices by JAX's collectives and lax.ppermute only.
A program may use at most 64 MiB of HBM per device.

v0:
```python
import jax
import jax.numpy as jnp
from jax import lax
from jax.sharding import PartitionSpec as P


def low_term(saved, cotangent, basis):
    reduced = jnp.dot(saved, basis, preferred_element_type=jnp.float32).astype(jnp.bfloat16)
    return lax.dot_general(
        reduced, cotangent, (((0,), (0,)), ((), ())), preferred_element_type=jnp.float32
    )


def moments(first, second, grad):
    first_new = 0.8 * first + 0.2 * grad
    second_new = 0.9 * second + 0.1 * grad * grad
    return (first_new, second_new, first_new / (jnp.sqrt(second_new) + 1e-08))


def weight_step(basis, direction, fs_count):
    row_count = basis.shape[0] // fs_count
    rows_here = lax.dynamic_slice_in_dim(basis, lax.axis_index("fs") * row_count, row_count, 0)
    return -jnp.dot(rows_here.astype(jnp.float32), direction, precision=lax.Precision.HIGHEST)


def body(
    in_saved,
    in_cotangent,
    point_saved,
    point_cotangent,
    in_basis,
    point_basis,
    in_first,
    in_second,
    point_first,
    point_second,
    in_master,
    point_master,
):
    fs_count = lax.axis_size("fs")
    in_low = low_term(in_saved, in_cotangent, in_basis)
    point_low = low_term(point_saved, point_cotangent, point_basis)
    rank_rows = in_low.shape[0]
    entries = 1.0 * rank_rows * (in_low.shape[1] + point_low.shape[1])
    part_in, part_point = (
        lax.psum_scatter(in_low, "tp", scatter_dimension=1, tiled=True),
        lax.psum_scatter(point_low, "tp", scatter_dimension=1, tiled=True),
    )
    sum_in, sum_point = lax.psum((part_in, part_point), "fs")
    squares = lax.psum(jnp.sum(sum_in * sum_in) + jnp.sum(sum_point * sum_point), "tp")
    clip_factor = jnp.minimum(1.0, 1.0 / jnp.sqrt(squares / entries + 1e-06))
    previous = (
        lax.all_gather(in_first, "fs", axis=0, tiled=True),
        lax.all_gather(in_second, "fs", axis=0, tiled=True),
        lax.all_gather(point_first, "fs", axis=0, tiled=True),
        lax.all_gather(point_second, "fs", axis=0, tiled=True),
    )
    in_first_all, in_second_all, in_direction = moments(
        previous[0], previous[1], clip_factor * sum_in
    )
    point_first_all, point_second_all, point_direction = moments(
        previous[2], previous[3], clip_factor * sum_point
    )
    row_count = rank_rows // fs_count
    row_start = lax.axis_index("fs") * row_count
    in_first_new = lax.dynamic_slice_in_dim(in_first_all, row_start, row_count, 0)
    in_second_new = lax.dynamic_slice_in_dim(in_second_all, row_start, row_count, 0)
    point_first_new = lax.dynamic_slice_in_dim(point_first_all, row_start, row_count, 0)
    point_second_new = lax.dynamic_slice_in_dim(point_second_all, row_start, row_count, 0)
    in_step = weight_step(in_basis, in_direction, fs_count)
    point_step = weight_step(point_basis, point_direction, fs_count)
    in_master_new = in_master + in_step
    point_master_new = point_master + point_step
    in_copy, point_copy = (
        lax.all_gather(in_master_new.astype(jnp.bfloat16), "fs", axis=0, tiled=True),
        lax.all_gather(point_master_new.astype(jnp.bfloat16), "fs", axis=0, tiled=True),
    )
    return (
        in_first_new,
        in_second_new,
        point_first_new,
        point_second_new,
        in_step,
        point_step,
        in_master_new,
        point_master_new,
        in_copy,
        point_copy,
    )


def solution(mesh):
    return jax.shard_map(
        body,
        mesh=mesh,
        in_specs=(
            P(("fs", "tp"), None),
            P(("fs", "tp"), None),
            P(("fs", "tp"), None),
            P(("fs", "tp"), None),
            P(),
            P(),
            P("fs", "tp"),
            P("fs", "tp"),
            P("fs", "tp"),
            P("fs", "tp"),
            P("fs", "tp"),
            P("fs", "tp"),
        ),
        out_specs=(
            P("fs", "tp"),
            P("fs", "tp"),
            P("fs", "tp"),
            P("fs", "tp"),
            P("fs", "tp"),
            P("fs", "tp"),
            P("fs", "tp"),
            P("fs", "tp"),
            P(None, "tp"),
            P(None, "tp"),
        ),
        check_vma=False,
    )
```

profile of v0, /device:TPU:0, one launch (start us, length us, event | category | flops | bytes accessed | tf_op | source)
XLA Modules:
  0.0 221.0 jit_solution(17097462439443650107)
XLA Ops:
  7.3 1.0 copy-done
  8.3 2.9 %fusion = f32[128,2048]{1,0:T(8,128)} fusion(bf16[192,2048]{1,0:T(8,128)(2,1)S(1)} %copy-done, bf16[192,2048]{1,0:T(8,128)(2,1)} %param.12, bf16[2048,128]{1,0:T(8,128)(2,1)} %param.16), kind=kOutput, calls=%fused_computation.4 | convolution fusion | flops 201351168 | bytes 3145728 | tf_op jit(solution)/shard_map/dot_general | solution.py:9
  11.4 1.6 fusion.1
  13.1 15.9 %all_gather.18 = f32[128,512]{1,0:T(8,128)S(1)} all-gather(f32[16,512]{1,0:T(8,128)S(1)} %copy-done.6), channel_id=1, replica_groups=mesh['fs'=8,'tp'=4] {'fs'}, dimensions={0}, use_global_device_ids=true | all-gather | bytes 294912 | tf_op jit(solution)/shard_map/all_gather | solution.py:53
  29.0 13.2 %reduce-scatter.3.cloned.1.call-done = f32[128,512]{1,0:T(8,128)} async-done(((f32[128,2048]{1,0:T(8,128)}), f32[128,512]{1,0:T(8,128)}) %reduce-scatter.3.cloned.1.call-update) | async-done | bytes 262160 | tf_op jit(solution)/shard_map/reduce_scatter | solution.py:46
  42.2 31.4 %reduce-scatter.5.cloned.1.call-done = f32[128,512]{1,0:T(8,128)} async-done(((f32[128,2048]{1,0:T(8,128)}), f32[128,512]{1,0:T(8,128)}) %reduce-scatter.5.cloned.1.call-update) | async-done | bytes 262160 | tf_op jit(solution)/shard_map/reduce_scatter | solution.py:47
  73.7 14.4 %all_gather.19 = f32[128,512]{1,0:T(8,128)S(1)} all-gather(f32[16,512]{1,0:T(8,128)S(1)} %copy-done.7), channel_id=1, replica_groups=mesh['fs'=8,'tp'=4] {'fs'}, dimensions={0}, use_global_device_ids=true | all-gather | bytes 294912 | tf_op jit(solution)/shard_map/all_gather | solution.py:54
  88.1 14.5 %all_gather.20 = f32[128,512]{1,0:T(8,128)S(1)} all-gather(f32[16,512]{1,0:T(8,128)S(1)} %copy-done.8), channel_id=1, replica_groups=mesh['fs'=8,'tp'=4] {'fs'}, dimensions={0}, use_global_device_ids=true | all-gather | bytes 294912 | tf_op jit(solution)/shard_map/all_gather | solution.py:55
  102.6 14.4 %all_gather.21 = f32[128,512]{1,0:T(8,128)S(1)} all-gather(f32[16,512]{1,0:T(8,128)S(1)} %copy-done.9), channel_id=1, replica_groups=mesh['fs'=8,'tp'=4] {'fs'}, dimensions={0}, use_global_device_ids=true | all-gather | bytes 294912 | tf_op jit(solution)/shard_map/all_gather | solution.py:56
  117.1 16.2 %all-reduce.3.cloned.1.call-done = (f32[128,512]{1,0:T(8,128)}, f32[128,512]{1,0:T(8,128)}) async-done(((f32[128,512]{1,0:T(8,128)}, f32[128,512]{1,0:T(8,128)}), (f32[128,512]{1,0:T(8,128)}, f32[128,512]{1,0:T(8,128)})) %all-reduce.3.cloned.1.call-update) | async-done | bytes 524304 | tf_op jit(solution)/shard_map/psum | solution.py:49
  133.3 1.6 multiply_reduce_fusion
  134.9 1.6 multiply_reduce_fusion.1
  137.8 10.2 %psum.23 = f32[]{:T(128)} all-reduce(f32[]{:T(128)S(6)} %add.50), channel_id=1, replica_groups=mesh['fs'=8,'tp'=4] {'tp'}, use_global_device_ids=true, to_apply=%region_6.0 | all-reduce | flops 1 | bytes 8 | tf_op jit(solution)/shard_map/psum | solution.py:50
  148.7 1.2 fusion.2
  150.0 2.7 %fusion.18 = (bf16[256,512]{1,0:T(8,128)(2,1)}, f32[256,512]{1,0:T(8,128)}, f32[256,512]{1,0:T(8,128)}) fusion(f32[256,512]{1,0:T(8,128)} %param.23, f32[128,512]{1,0:T(8,128)S(1)} %get-tuple-element.22, f32[128,512]{1,0:T(8,128)S(1)} %get-tuple-element.23, bf16[2048,128]{1,0:T(8,128)(2,1)S(1)} %copy-done.4, s32[]{:T(128)S(6)} %select_n.5), kind=kOutput, calls=%fused_computation.32 | convolution fusion | flops 201850880 | bytes 2424836 | tf_op jit(solution)/shard_map/dot_general | solution.py:23
  152.7 2.4 %fusion.19 = (bf16[256,512]{1,0:T(8,128)(2,1)}, f32[256,512]{1,0:T(8,128)}, f32[256,512]{1,0:T(8,128)}) fusion(f32[256,512]{1,0:T(8,128)S(1)} %copy-done.5, f32[128,512]{1,0:T(8,128)S(1)} %get-tuple-element.19, f32[128,512]{1,0:T(8,128)S(1)} %get-tuple-element.18, bf16[2048,128]{1,0:T(8,128)(2,1)} %param.16, s32[]{:T(128)S(6)} %select_n.5), kind=kOutput, calls=%fused_computation.33 | convolution fusion | flops 201850880 | bytes 2424836 | tf_op jit(solution)/shard_map/dot_general | solution.py:23
  155.1 0.6 constant_dynamic-slice_fusion.2
  155.8 0.6 constant_dynamic-slice_fusion.3
  156.4 0.6 constant_dynamic-slice_fusion.1
  157.0 0.6 constant_dynamic-slice_fusion
  157.6 21.7 %all-gather.5.cloned.1.call-done = bf16[2048,512]{1,0:T(8,128)(2,1)} async-done(((bf16[256,512]{1,0:T(8,128)(2,1)}), bf16[2048,512]{1,0:T(8,128)(2,1)}) %all-gather.5.cloned.1.call-update) | async-done | bytes 2097168 | tf_op jit(solution)/shard_map/all_gather | solution.py:76
  179.3 30.6 %all-gather.3.cloned.1.call-done = bf16[2048,512]{1,0:T(8,128)(2,1)} async-done(((bf16[256,512]{1,0:T(8,128)(2,1)}), bf16[2048,512]{1,0:T(8,128)(2,1)}) %all-gather.3.cloned.1.call-update) | async-done | bytes 2097168 | tf_op jit(solution)/shard_map/all_gather | solution.py:75
  209.9 3.2 %copy.26 = bf16[2048,512]{1,0:T(8,128)(2,1)} copy(bf16[2048,512]{1,0:T(8,128)(2,1)} %all-gather.3.cloned.1.call-done) | data formatting | bytes 4194304
  213.1 1.3 copy.27
  (29 shorter events, 0.3 us)
Async XLA Ops:
  7.2 1.1 copy-start
  7.2 4.2 %copy-start.4 = (bf16[2048,128]{1,0:T(8,128)(2,1)S(1)}, bf16[2048,128]{1,0:T(8,128)(2,1)}, u32[]{:S(2)}) copy-start(bf16[2048,128]{1,0:T(8,128)(2,1)} %param.17) | copy-start | bytes 1572868
  7.2 4.2 %copy-start.2 = (bf16[192,2048]{1,0:T(8,128)(2,1)S(1)}, bf16[192,2048]{1,0:T(8,128)(2,1)}, u32[]{:S(2)}) copy-start(bf16[192,2048]{1,0:T(8,128)(2,1)} %param.15) | copy-start | bytes 2359300
  7.2 4.2 %copy-start.3 = (bf16[192,2048]{1,0:T(8,128)(2,1)S(1)}, bf16[192,2048]{1,0:T(8,128)(2,1)}, u32[]{:S(2)}) copy-start(bf16[192,2048]{1,0:T(8,128)(2,1)} %param.14) | copy-start | bytes 2359300
  7.2 35.0 %reduce-scatter.3.cloned.1.call-start = ((), (), s32[]{:S(2)}) async-start(), calls=%async_computation.2 | async-start | bytes 1310720 | tf_op jit(solution)/shard_map/reduce_scatter | solution.py:46
  11.3 1.9 copy-start.6
  11.3 62.4 %copy-start.7 = (f32[16,512]{1,0:T(8,128)S(1)}, f32[16,512]{1,0:T(8,128)}, u32[]{:S(2)}) copy-start(f32[16,512]{1,0:T(8,128)} %param.19) | copy-start | bytes 98308
  11.3 76.8 %copy-start.8 = (f32[16,512]{1,0:T(8,128)S(1)}, f32[16,512]{1,0:T(8,128)}, u32[]{:S(2)}) copy-start(f32[16,512]{1,0:T(8,128)} %param.20) | copy-start | bytes 98308
  11.3 91.3 %copy-start.9 = (f32[16,512]{1,0:T(8,128)S(1)}, f32[16,512]{1,0:T(8,128)}, u32[]{:S(2)}) copy-start(f32[16,512]{1,0:T(8,128)} %param.21) | copy-start | bytes 98308
  11.3 62.3 %reduce-scatter.5.cloned.1.call-start = ((), (), s32[]{:S(2)}) async-start(), calls=%async_computation.3 | async-start | bytes 1310720 | tf_op jit(solution)/shard_map/reduce_scatter | solution.py:47
  13.1 120.2 %all-reduce.3.cloned.1.call-start = ((), (), s32[]{:S(2)}) async-start(), calls=%async_computation.6 | async-start | bytes 1048576 | tf_op jit(solution)/shard_map/psum | solution.py:49
  73.6 105.7 %all-gather.5.cloned.1.call-start = ((), (), s32[]{:S(2)}) async-start(), calls=%async_computation.5 | async-start | bytes 2359296 | tf_op jit(solution)/shard_map/all_gather | solution.py:76
  149.9 2.8 %copy-start.5 = (f32[256,512]{1,0:T(8,128)S(1)}, f32[256,512]{1,0:T(8,128)}, u32[]{:S(2)}) copy-start(f32[256,512]{1,0:T(8,128)} %param.22) | copy-start | bytes 1572868
  152.6 57.3 %all-gather.3.cloned.1.call-start = ((), (), s32[]{:S(2)}) async-start(), calls=%async_computation.4 | async-start | bytes 2359296 | tf_op jit(solution)/shard_map/all_gather | solution.py:75
  209.9 3.2 %copy-start.1 = (bf16[2048,512]{1,0:T(8,128)(2,1)S(1)}, bf16[2048,512]{1,0:T(8,128)(2,1)}, u32[]{:S(2)}) copy-start(bf16[2048,512]{1,0:T(8,128)(2,1)} %all-gather.5.cloned.1.call-done) | copy-start | bytes 6291460
Sparse Core Ops, SparseCore 0:
  11.5 30.6 reduce-scatter.2
  45.7 27.9 reduce-scatter.4
  76.0 57.2 all-reduce.2
  152.8 26.5 all-gather.4
  181.4 28.5 all-gather.2
where the time goes:
time: 221 us
  waiting for transfers between devices  113 us (51%)
  blocking collectives  69.4 us (31%)
  between operations  15.9 us (7%)
  matrix products  9.64 us (4%)
  local copies, waits for them, and re-layouts  8.09 us (4%)
  other arithmetic  4.47 us (2%)
    reduce_scatter x1, waiting for transfers between devices, body(): lax.psum_scatter(point_low, 'tp', scatter_dimension=1, tiled=True)  31.4 us
    all_gather x1, waiting for transfers between devices, body(): lax.all_gather(in_master_new.astype(jnp.bfloat16), 'fs', axis=0, tiled=True)  30.6 us
    all_gather x1, waiting for transfers between devices, body(): lax.all_gather(point_master_new.astype(jnp.bfloat16), 'fs', axis=0, tiled...  21.7 us
    psum x1, waiting for transfers between devices, body(): sum_in, sum_point = lax.psum((part_in, part_point), 'fs')  16.2 us
    all_gather x1, blocking collectives, body(): lax.all_gather(in_first, 'fs', axis=0, tiled=True)  15.9 us
    all_gather x1, blocking collectives, body(): lax.all_gather(point_first, 'fs', axis=0, tiled=True)  14.5 us
    all_gather x1, blocking collectives, body(): lax.all_gather(point_second, 'fs', axis=0, tiled=True)  14.4 us
    all_gather x1, blocking collectives, body(): lax.all_gather(in_second, 'fs', axis=0, tiled=True)  14.4 us
  transfers between devices with their start and end apart: 5, of which 5 were waited for; matrix products, arithmetic and copies ran while one was open for 3% of the time, Pallas kernels for 0%

commit v1 on v0

v1 whole, which is shorter than its diff:
```python
import jax
import jax.numpy as jnp
from jax import lax
from jax.experimental import pallas as pl
from jax.experimental.pallas import tpu as pltpu
from jax.sharding import PartitionSpec as P


CORES = 2


def low_term(saved, cotangent, basis):
    reduced = jnp.dot(saved, basis, preferred_element_type=jnp.float32).astype(jnp.bfloat16)
    return lax.dot_general(
        reduced, cotangent, (((0,), (0,)), ((), ())), preferred_element_type=jnp.float32
    )


def moments(first, second, grad):
    first_new = 0.8 * first + 0.2 * grad
    second_new = 0.9 * second + 0.1 * grad * grad
    return (first_new, second_new, first_new / (jnp.sqrt(second_new) + 1e-08))


def weight_step(basis, direction, fs_count):
    row_count = basis.shape[0] // fs_count
    rows_here = lax.dynamic_slice_in_dim(basis, lax.axis_index("fs") * row_count, row_count, 0)
    return -jnp.dot(rows_here.astype(jnp.float32), direction, precision=lax.Precision.HIGHEST)


def clip_of(squares, entries):
    return jnp.minimum(1.0, 1.0 / jnp.sqrt(squares / entries + 1e-06))


def plain_body(
    in_saved,
    in_cotangent,
    point_saved,
    point_cotangent,
    in_basis,
    point_basis,
    in_first,
    in_second,
    point_first,
    point_second,
    in_master,
    point_master,
):
    fs_count = lax.axis_size("fs")
    in_low = low_term(in_saved, in_cotangent, in_basis)
    point_low = low_term(point_saved, point_cotangent, point_basis)
    rank_rows = in_low.shape[0]
    entries = 1.0 * rank_rows * (in_low.shape[1] + point_low.shape[1])
    part_in, part_point = (
        lax.psum_scatter(in_low, "tp", scatter_dimension=1, tiled=True),
        lax.psum_scatter(point_low, "tp", scatter_dimension=1, tiled=True),
    )
    sum_in, sum_point = lax.psum((part_in, part_point), "fs")
    squares = lax.psum(jnp.sum(sum_in * sum_in) + jnp.sum(sum_point * sum_point), "tp")
    clip_factor = clip_of(squares, entries)
    previous = tuple(
        lax.all_gather(a, "fs", axis=0, tiled=True)
        for a in (in_first, in_second, point_first, point_second)
    )
    in_first_all, in_second_all, in_direction = moments(
        previous[0], previous[1], clip_factor * sum_in
    )
    point_first_all, point_second_all, point_direction = moments(
        previous[2], previous[3], clip_factor * sum_point
    )
    row_count = rank_rows // fs_count
    row_start = lax.axis_index("fs") * row_count
    mine = tuple(
        lax.dynamic_slice_in_dim(a, row_start, row_count, 0)
        for a in (in_first_all, in_second_all, point_first_all, point_second_all)
    )
    in_step = weight_step(in_basis, in_direction, fs_count)
    point_step = weight_step(point_basis, point_direction, fs_count)
    in_master_new = in_master + in_step
    point_master_new = point_master + point_step
    in_copy, point_copy = (
        lax.all_gather(in_master_new.astype(jnp.bfloat16), "fs", axis=0, tiled=True),
        lax.all_gather(point_master_new.astype(jnp.bfloat16), "fs", axis=0, tiled=True),
    )
    return (*mine, in_step, point_step, in_master_new, point_master_new, in_copy, point_copy)


def exchange(x, fs_mask, tp_mask=0):
    fs_count, tp_count = lax.axis_size("fs"), lax.axis_size("tp")
    pairs = [
        (f * tp_count + t, (f ^ fs_mask) * tp_count + (t ^ tp_mask))
        for f in range(fs_count)
        for t in range(tp_count)
    ]
    return lax.ppermute(x, ("fs", "tp"), pairs)


PLAIN_UNIT = 2.0**-14
VMEM = pl.BlockSpec(memory_space=pltpu.VMEM)
HBM = pl.BlockSpec(memory_space=pltpu.HBM)
TAG = 8


def shape(*dims, dtype=jnp.float32):
    return jax.ShapeDtypeStruct(dims, dtype)


def code(y):
    y2 = y * y
    y4 = y2 * y2
    y8 = y4 * y4
    return jnp.where(y < 0.0, -y8, y8).astype(jnp.bfloat16)


def uncode(t):
    t = t.astype(jnp.float32)
    size = jnp.exp2(jnp.log2(jnp.abs(t)) * 0.125)
    return jnp.where(t < 0.0, -size, size)


def unit_for(largest):
    unit = jnp.maximum(largest, 1e-30) * (1.0156 * 2.0**-15.75)
    return unit.astype(jnp.bfloat16)


def call(kernel, outs, args, mib, hbm_args=False, hbm_outs=False, scratch=()):
    return pl.pallas_call(
        kernel,
        out_shape=outs,
        in_specs=[HBM if hbm_args else VMEM] * len(args),
        out_specs=[HBM if hbm_outs else VMEM] * len(outs),
        scratch_shapes=scratch,
        compiler_params=pltpu.CompilerParams(vmem_limit_bytes=mib << 20),
    )(*args)


def begin(stored, saved, cotangents, bases):
    rank, width = bases[0].shape[1], cotangents[0].shape[1]
    cols = stored[0][0].shape[1]
    packed = sum(a.shape[0] for a in stored[0])
    first = len(stored[0])
    arrays = (*stored[0], *stored[1], bases[0], saved[0], cotangents[0], bases[1], saved[1], cotangents[1])
    count = len(arrays)

    def kernel(*refs):
        sources, outs = refs[:count], refs[count : count + 4]
        held, sems = refs[count + 4 : 2 * count + 4], refs[2 * count + 4]
        core = lax.axis_index("fs") % CORES
        copies = [
            pltpu.make_async_copy(src, dst, sems.at[n])
            for n, (src, dst) in enumerate(zip(sources, held))
        ]
        for copy in copies:
            copy.start()
        for which in range(2):
            row = 0
            for n in range(which * first, (which + 1) * first):
                copies[n].wait()
                size = held[n].shape[0]
                outs[which][row : row + size, :] = code(held[n][...] * (1.0 / PLAIN_UNIT))
                row += size
        for which in range(2):
            at = 2 * first + 3 * which
            copies[at].wait()
            copies[at + 1].wait()
            reduced = jnp.dot(
                held[at + 1][...], held[at][...], preferred_element_type=jnp.float32
            )
            copies[at + 2].wait()
            term = lax.dot_general(
                reduced.astype(jnp.bfloat16),
                held[at + 2][...],
                (((0,), (0,)), ((), ())),
                preferred_element_type=jnp.float32,
            )

            @pl.when(core == which)
            def _():
                outs[3][...] = term

            @pl.when(core != which)
            def _():
                outs[2][...] = term

    scratch = [pltpu.VMEM(a.shape, a.dtype) for a in arrays] + [pltpu.SemaphoreType.DMA((count,))]
    outs = [shape(packed, cols, dtype=jnp.bfloat16)] * 2 + [shape(rank, width)] * 2
    return call(kernel, outs, arrays, 60, hbm_args=True, scratch=scratch)


def put_coded(ref, value, unit):
    rank = value.shape[0]
    ref[:rank, :] = code(value * (1.0 / unit.astype(jnp.float32)))
    ref[rank:, :] = jnp.full((TAG, ref.shape[1]), unit, jnp.bfloat16)


def get_coded(ref):
    rank = ref.shape[0] - TAG
    return uncode(ref[:rank, :]) * ref[rank:, :].astype(jnp.float32)[:1, :1]


def chip_sum(keep, given, count):
    rank, width = keep.shape
    cols = width // count

    def kernel(keep, given, mine, *rest):
        coded, total = rest[:-1], rest[-1]
        column = lax.axis_index("tp")
        value = keep[...] + given[...]
        total[...] = value
        unit = unit_for(jnp.max(jnp.abs(value)))
        mine[...] = total[:, pl.ds(pl.multiple_of(column * cols, cols), cols)]
        for k in range(1, count):
            at = pl.multiple_of((column ^ k) * cols, cols)
            put_coded(coded[k - 1], total[:, pl.ds(at, cols)], unit)

    outs = [shape(rank, cols)] + [shape(rank + TAG, cols, dtype=jnp.bfloat16)] * (count - 1)
    scratch = [pltpu.VMEM((rank, width), jnp.float32)]
    return call(kernel, outs, (keep, given), 8, scratch=scratch)


def plane_sum(mine, got):
    def kernel(mine, *refs):
        value = mine[...]
        for ref in refs[:-1]:
            value = value + get_coded(ref)
        put_coded(refs[-1], value, unit_for(jnp.max(jnp.abs(value))))

    outs = [shape(mine.shape[0] + TAG, mine.shape[1], dtype=jnp.bfloat16)]
    return call(kernel, outs, (mine, *got), 8)[0]


def pair_sum(a, b, last):
    def kernel(a, b, out):
        value = get_coded(a) + get_coded(b)
        if last:
            out[...] = value
        else:
            put_coded(out, value, unit_for(jnp.max(jnp.abs(value))))

    rows, cols = a.shape
    out = shape(rows - TAG, cols) if last else shape(rows, cols, dtype=a.dtype)
    return call(kernel, [out], (a, b), 8)[0]


def square_sum(a, b):
    def kernel(a, b, out):
        value = jnp.sum(a[...] * a[...]) + jnp.sum(b[...] * b[...])
        out[...] = jnp.full(out.shape, value, jnp.float32)

    return call(kernel, [shape(8, 128)], (a, b), 4)[0]


def finish(entries, total, other, squares, bases, masters, old, blocks):
    rows, cols = masters[0].shape
    full, rank = bases[0].shape
    here = old[0].shape[0]
    n_sq, n_bl = len(squares), len(blocks)

    def kernel(*refs):
        refs = list(refs)

        def take(n):
            part = refs[:n]
            del refs[:n]
            return part

        total, other = take(2)
        square_refs = take(n_sq)
        basis_refs = take(2)
        master_refs = take(2)
        old_refs = take(4)
        block_refs = [take(2) for _ in range(n_bl)]
        outs = take(10)
        grads, direction, small, own, stage, sems = refs
        me = lax.axis_index("fs")
        core = me % CORES
        copies = []

        def send(src, dst):
            copies.append(pltpu.make_async_copy(src, dst, sems.at[len(copies)]))
            copies[-1].start()

        squares = square_refs[0][...]
        for ref in square_refs[1:]:
            squares = squares + ref[...]
        clip = clip_of(squares[:1, :1], entries)
        mine = total[...] * clip
        theirs = other[...] * clip
        grads[0] = jnp.where(core == 0, mine, theirs)
        grads[1] = jnp.where(core == 0, theirs, mine)
        for which in range(2):
            grad = grads[which, pl.ds(pl.multiple_of(me * here, here), here), :]
            new = moments(old_refs[2 * which][...], old_refs[2 * which + 1][...], grad)
            for j in range(2):
                small[2 * which + j] = new[j]
                send(small.at[2 * which + j], outs[2 * which + j])
        for n in range(n_bl):
            at = pl.multiple_of((me ^ n) * here, here)
            for which in range(2):
                ref = block_refs[n][which]
                first = uncode(ref[rows : rows + here, :]) * PLAIN_UNIT
                second = uncode(ref[rows + here : rows + 2 * here, :]) * PLAIN_UNIT
                value = moments(first, second, grads[which, pl.ds(at, here), :])[2]
                high = value.astype(jnp.bfloat16)
                direction[which, pl.ds(at, here), :] = high
                direction[which, pl.ds(pl.multiple_of(rank + at, here), here), :] = (
                    value - high.astype(jnp.float32)
                ).astype(jnp.bfloat16)

        for n in range(n_bl):
            row0 = pl.multiple_of((me ^ n) * rows, rows)
            for which in range(2):
                b = basis_refs[which][pl.ds(row0, rows), :]
                both = jnp.concatenate([b, b], axis=1)
                down = jnp.dot(both, direction[which], preferred_element_type=jnp.float32)
                if n == 0:
                    own[which] = -down
                    own[2 + which] = master_refs[which][...] - down
                    for j in (which, 2 + which):
                        send(own.at[j], outs[4 + j])
                value = uncode(block_refs[n][which][:rows, :]) * PLAIN_UNIT
                stage[2 * n + which] = (value - down).astype(jnp.bfloat16)
                send(stage.at[2 * n + which], outs[8 + which].at[pl.ds(row0, rows), :])
        for copy in copies:
            copy.wait()

    outs = [shape(here, cols)] * 4 + [shape(rows, cols)] * 4
    outs += [shape(full, cols, dtype=jnp.bfloat16)] * 2
    flat = [array for block in blocks for array in block]
    args = (total, other, *squares, *bases, *masters, *old, *flat)
    scratch = [
        pltpu.VMEM((2, rank, cols), jnp.float32),
        pltpu.VMEM((2, 2 * rank, cols), jnp.bfloat16),
        pltpu.VMEM((4, here, cols), jnp.float32),
        pltpu.VMEM((4, rows, cols), jnp.float32),
        pltpu.VMEM((2 * n_bl, rows, cols), jnp.bfloat16),
        pltpu.SemaphoreType.DMA((8 + 2 * n_bl,)),
    ]
    return call(kernel, outs, args, 24, hbm_outs=True, scratch=scratch)


def short_body(
    in_saved,
    in_cotangent,
    point_saved,
    point_cotangent,
    in_basis,
    point_basis,
    in_first,
    in_second,
    point_first,
    point_second,
    in_master,
    point_master,
):
    tp_count = lax.axis_size("tp")
    rank = in_basis.shape[1]
    entries = 1.0 * rank * (in_cotangent.shape[1] + point_cotangent.shape[1])
    masters = (in_master, point_master)
    old = (in_first, in_second, point_first, point_second)
    bases = (in_basis, point_basis)

    *packs, give, keep = begin(
        ((in_master, in_first, in_second), (point_master, point_first, point_second)),
        (in_saved, point_saved),
        (in_cotangent, point_cotangent),
        bases,
    )
    given = exchange(give, 1)
    one = [exchange(p, CORES) for p in packs]
    three = [exchange(p, 3 * CORES) for p in packs]

    mine, *coded = chip_sum(keep, given, tp_count)
    got = [exchange(coded[k - 1], 0, k) for k in range(1, tp_count)]
    coded = plane_sum(mine, got)
    coded = pair_sum(coded, exchange(coded, CORES), False)
    total = pair_sum(coded, exchange(coded, 2 * CORES), True)
    two = [exchange(t, CORES) for t in three]
    other = exchange(total, 1)
    squares = square_sum(total, other)
    squares = [squares] + [exchange(squares, 0, k) for k in range(1, tp_count)]
    blocks = []
    for arrays in (packs, one, two, three):
        swapped = [exchange(a, 1) for a in arrays]
        blocks += [arrays, swapped]
    return tuple(finish(entries, total, other, squares, bases, masters, old, blocks))


def solution(mesh):
    z_count = mesh.shape["fs"] // CORES
    tp_count = mesh.shape["tp"]
    short = z_count == 4 and tp_count == 4
    return jax.shard_map(
        short_body if short else plain_body,
        mesh=mesh,
        in_specs=(P(("fs", "tp"), None),) * 4 + (P(),) * 2 + (P("fs", "tp"),) * 6,
        out_specs=(P("fs", "tp"),) * 8 + (P(None, "tp"),) * 2,
        check_vma=False,
    )
```

time: 221 us -> 75.9 us (0.34)
  waiting for transfers between devices: 113 us -> 33.9 us
  blocking collectives: 69.4 us -> 0 us
  starting transfers between devices: 0.2 us -> 27.9 us
  between operations: 15.9 us -> 0.84 us
  Pallas kernels: 0 us -> 11.8 us
  matrix products: 9.64 us -> 0 us
  local copies, waits for them, and re-layouts: 8.09 us -> 1.28 us
  other arithmetic: 4.47 us -> 0 us
    all_gather x4 -> x0, blocking collectives: 59.2 us -> none  [the longest x1 15.9 us: body(): lax.all_gather(in_first, 'fs', axis=0, tiled=True)]
    all_gather x2 -> x0, waiting for transfers between devices: 52.3 us -> none  [the longest x1 30.6 us: body(): lax.all_gather(in_master_new.astype(jnp.bfloat16), 'fs', axis=0, tiled=True)]
    reduce_scatter x2 -> x0, waiting for transfers between devices: 44.6 us -> none  [the longest x1 31.4 us: body(): lax.psum_scatter(point_low, 'tp', scatter_dimension=1, tiled=True)]
    ppermute x0 -> x24, waiting for transfers between devices: none -> 33.9 us  [exchange(): return lax.ppermute(x, ('fs', 'tp'), pairs)]
    ppermute x0 -> x24, starting transfers between devices: none -> 27.9 us  [exchange(): return lax.ppermute(x, ('fs', 'tp'), pairs)]
    psum x1 -> x0, waiting for transfers between devices: 16.2 us -> none  [body(): sum_in, sum_point = lax.psum((part_in, part_point), 'fs')]
    pallas_call x0 -> x7, Pallas kernels: none -> 11.8 us  [call(): pl.pallas_call(kernel, out_shape=outs, in_specs=[HBM if hbm_args else VME...]
    psum x1 -> x0, blocking collectives: 10.2 us -> none  [body(): lax.psum(jnp.sum(sum_in * sum_in) + jnp.sum(sum_point * sum_point), 'tp')]
  transfers between devices with their start and end apart: 5 -> 24, of which waited for: 5 -> 11; matrix products, arithmetic and copies ran while one was open for 3% -> 0% of each run, Pallas kernels for 0% -> 2%
where the time goes in v1:
time: 75.9 us; the launch traced here: 75.7 us
  waiting for transfers between devices  33.9 us (45%)
  starting transfers between devices  27.9 us (37%)
  Pallas kernels  11.8 us (16%)
  local copies, waits for them, and re-layouts  1.28 us (2%)
  between operations  0.84 us (1%)
    ppermute x24, waiting for transfers between devices, exchange(): return lax.ppermute(x, ('fs', 'tp'), pairs)  33.9 us
    ppermute x24, starting transfers between devices, exchange(): return lax.ppermute(x, ('fs', 'tp'), pairs)  27.9 us
    pallas_call x7, Pallas kernels, call(): pl.pallas_call(kernel, out_shape=outs, in_specs=[HBM if hbm_args else VME...  11.8 us
  transfers between devices with their start and end apart: 24, of which 11 were waited for; matrix products, arithmetic and copies ran while one was open for 0% of the time, Pallas kernels for 2%

profile of v1, /device:TPU:0, one launch (start us, length us, event | category | flops | bytes accessed | tf_op | source)
XLA Modules:
  0.0 75.7 jit_solution(5731489683757445781)
XLA Ops:
  0.6 4.8 %shard_map.195 = (bf16[288,512]{1,0:T(8,128)(2,1)}, bf16[288,512]{1,0:T(8,128)(2,1)}, f32[128,2048]{1,0:T(8,128)}, f32[128,2048]{1,0:T(8,128)}) custom-call(f32[256,512]{1,0:T(8,128)} %refs_8_.3, f32[16,512]{1,0:T(8,128)} %refs_10_.3, f32[16,512]{1,0:T(8,128)} %refs_11_.3, f32[256,512]{1,0:T(8,128)} %refs_9_.3, f32[16,512]{1,0:T(8,128)} %refs_12_.1, ...), custom_call_target="tpu_custom_call" | custom-call | tf_op jit(solution)/shard_map/pallas_call | solution.py:127
  6.0 2.5 %collective-permute-done.given = f32[128,2048]{1,0:T(8,128)S(1)} collective-permute-done((f32[128,2048]{1,0:T(8,128)}, f32[128,2048]{1,0:T(8,128)S(1)}, u32[]{:S(2)}, u32[]{:S(2)}) %collective-permute-start) | collective-permute-done | bytes 1048608 | tf_op jit(solution)/shard_map/ppermute | solution.py:95
  8.5 1.2 %copy-done.4 = f32[128,2048]{1,0:T(8,128)S(1)} copy-done((f32[128,2048]{1,0:T(8,128)S(1)}, f32[128,2048]{1,0:T(8,128)}, u32[]{:S(2)}) %copy-start.4) | copy-done | bytes 1048600
  9.8 0.6 shard_map.196
  10.4 2.9 %collective-permute-start.1 = (bf16[136,512]{1,0:T(8,128)(2,1)S(1)}, bf16[136,512]{1,0:T(8,128)(2,1)S(1)}, u32[]{:S(2)}, u32[]{:S(2)}) collective-permute-start(bf16[136,512]{1,0:T(8,128)(2,1)S(1)} %get-tuple-element.21), channel_id=1, source_target_pairs={{0,1},{1,0},{2,3},{3,2},{4,5},{5,4},{6,7},{7,6},{8,9},{9,8},{10,11... | collective-permute-start | bytes 417800 | tf_op jit(solution)/shard_map/ppermute | solution.py:95
  13.3 1.5 %collective-permute-start.2 = (bf16[136,512]{1,0:T(8,128)(2,1)S(1)}, bf16[136,512]{1,0:T(8,128)(2,1)S(1)}, u32[]{:S(2)}, u32[]{:S(2)}) collective-permute-start(bf16[136,512]{1,0:T(8,128)(2,1)S(1)} %get-tuple-element.22), channel_id=1, source_target_pairs={{0,2},{1,3},{2,0},{3,1},{4,6},{5,7},{6,4},{7,5},{8,10},{9,11},{10,... | collective-permute-start | bytes 417800 | tf_op jit(solution)/shard_map/ppermute | solution.py:95
  14.9 4.0 %collective-permute-start.16 = (bf16[288,512]{1,0:T(8,128)(2,1)}, bf16[288,512]{1,0:T(8,128)(2,1)S(1)}, u32[]{:S(2)}, u32[]{:S(2)}) collective-permute-start(bf16[288,512]{1,0:T(8,128)(2,1)} %get-tuple-element.24.refs_14_), channel_id=1, source_target_pairs={{0,24},{1,25},{2,26},{3,27},{4,28},{5,29},{6,30},{7,31},{8,16},{9,... | collective-permute-start | bytes 884744 | tf_op jit(solution)/shard_map/ppermute | solution.py:95
  18.9 2.8 %collective-permute-done.2.refs_1_ = bf16[136,512]{1,0:T(8,128)(2,1)S(1)} collective-permute-done((bf16[136,512]{1,0:T(8,128)(2,1)S(1)}, bf16[136,512]{1,0:T(8,128)(2,1)S(1)}, u32[]{:S(2)}, u32[]{:S(2)}) %collective-permute-start.2) | collective-permute-done | bytes 139296 | tf_op jit(solution)/shard_map/ppermute | solution.py:95
  22.3 1.6 %collective-permute-start.4 = (bf16[136,512]{1,0:T(8,128)(2,1)S(1)}, bf16[136,512]{1,0:T(8,128)(2,1)S(1)}, u32[]{:S(2)}, u32[]{:S(2)}) collective-permute-start(bf16[136,512]{1,0:T(8,128)(2,1)S(1)} %shard_map.197.a), channel_id=1, source_target_pairs={{0,8},{1,9},{2,10},{3,11},{4,12},{5,13},{6,14},{7,15},{8,0},{9,1},... | collective-permute-start | bytes 417800 | tf_op jit(solution)/shard_map/ppermute | solution.py:95
  24.4 3.6 %collective-permute-start.18 = (bf16[288,512]{1,0:T(8,128)(2,1)S(1)}, bf16[288,512]{1,0:T(8,128)(2,1)S(1)}, u32[]{:S(2)}, u32[]{:S(2)}) collective-permute-start(bf16[288,512]{1,0:T(8,128)(2,1)S(1)} %copy-done.6), channel_id=1, source_target_pairs={{0,24},{1,25},{2,26},{3,27},{4,28},{5,29},{6,30},{7,31},{8,16},{9,... | collective-permute-start | bytes 884744 | tf_op jit(solution)/shard_map/ppermute | solution.py:95
  28.0 1.5 %collective-permute-done.4.b = bf16[136,512]{1,0:T(8,128)(2,1)S(1)} collective-permute-done((bf16[136,512]{1,0:T(8,128)(2,1)S(1)}, bf16[136,512]{1,0:T(8,128)(2,1)S(1)}, u32[]{:S(2)}, u32[]{:S(2)}) %collective-permute-start.4) | collective-permute-done | bytes 139296 | tf_op jit(solution)/shard_map/ppermute | solution.py:95
  29.5 2.5 %collective-permute-start.13 = (bf16[288,512]{1,0:T(8,128)(2,1)S(1)}, bf16[288,512]{1,0:T(8,128)(2,1)S(1)}, u32[]{:S(2)}, u32[]{:S(2)}) collective-permute-start(bf16[288,512]{1,0:T(8,128)(2,1)S(1)} %copy-done.6), channel_id=1, source_target_pairs={{0,8},{1,9},{2,10},{3,11},{4,12},{5,13},{6,14},{7,15},{8,0},{9,1},... | collective-permute-start | bytes 884744 | tf_op jit(solution)/shard_map/ppermute | solution.py:95
  32.4 1.9 %collective-permute-start.5 = (bf16[136,512]{1,0:T(8,128)(2,1)S(1)}, bf16[136,512]{1,0:T(8,128)(2,1)S(1)}, u32[]{:S(2)}, u32[]{:S(2)}) collective-permute-start(bf16[136,512]{1,0:T(8,128)(2,1)S(1)} %shard_map.198.a), channel_id=1, source_target_pairs={{0,16},{1,17},{2,18},{3,19},{4,20},{5,21},{6,22},{7,23},{8,24},{9,... | collective-permute-start | bytes 417800 | tf_op jit(solution)/shard_map/ppermute | solution.py:95
  34.3 2.6 %collective-permute-done.12.refs_18_ = bf16[288,512]{1,0:T(8,128)(2,1)S(1)} collective-permute-done((bf16[288,512]{1,0:T(8,128)(2,1)S(1)}, bf16[288,512]{1,0:T(8,128)(2,1)S(1)}, u32[]{:S(2)}, u32[]{:S(2)}) %collective-permute-start.12) | collective-permute-done | bytes 294944 | tf_op jit(solution)/shard_map/ppermute | solution.py:95
  37.5 6.1 %collective-permute-done.18.refs_27_ = bf16[288,512]{1,0:T(8,128)(2,1)S(1)} collective-permute-done((bf16[288,512]{1,0:T(8,128)(2,1)S(1)}, bf16[288,512]{1,0:T(8,128)(2,1)S(1)}, u32[]{:S(2)}, u32[]{:S(2)}) %collective-permute-start.18) | collective-permute-done | bytes 294944 | tf_op jit(solution)/shard_map/ppermute | solution.py:95
  43.6 1.6 %collective-permute-start.17 = (bf16[288,512]{1,0:T(8,128)(2,1)S(1)}, bf16[288,512]{1,0:T(8,128)(2,1)S(1)}, u32[]{:S(2)}, u32[]{:S(2)}) collective-permute-start(bf16[288,512]{1,0:T(8,128)(2,1)S(1)} %collective-permute-done.16.refs_26_), channel_id=1, source_target_pairs={{0,8},{1,9},{2,10},{3,11},{4,12},{5,13},{6,14},{7,15},{8,0},{9,1},... | collective-permute-start | bytes 884744 | tf_op jit(solution)/shard_map/ppermute | solution.py:95
  45.2 6.3 %collective-permute-done.5.b = bf16[136,512]{1,0:T(8,128)(2,1)S(1)} collective-permute-done((bf16[136,512]{1,0:T(8,128)(2,1)S(1)}, bf16[136,512]{1,0:T(8,128)(2,1)S(1)}, u32[]{:S(2)}, u32[]{:S(2)}) %collective-permute-start.5) | collective-permute-done | bytes 139296 | tf_op jit(solution)/shard_map/ppermute | solution.py:95
  51.5 2.0 %collective-permute-start.19 = (bf16[288,512]{1,0:T(8,128)(2,1)S(1)}, bf16[288,512]{1,0:T(8,128)(2,1)S(1)}, u32[]{:S(2)}, u32[]{:S(2)}) collective-permute-start(bf16[288,512]{1,0:T(8,128)(2,1)S(1)} %collective-permute-done.18.refs_27_), channel_id=1, source_target_pairs={{0,8},{1,9},{2,10},{3,11},{4,12},{5,13},{6,14},{7,15},{8,0},{9,1},... | collective-permute-start | bytes 884744 | tf_op jit(solution)/shard_map/ppermute | solution.py:95
  54.4 3.4 %collective-permute-done.17.refs_22_ = bf16[288,512]{1,0:T(8,128)(2,1)S(1)} collective-permute-done((bf16[288,512]{1,0:T(8,128)(2,1)S(1)}, bf16[288,512]{1,0:T(8,128)(2,1)S(1)}, u32[]{:S(2)}, u32[]{:S(2)}) %collective-permute-start.17) | collective-permute-done | bytes 294944 | tf_op jit(solution)/shard_map/ppermute | solution.py:95
  57.8 5.4 %collective-permute-done.19.refs_23_ = bf16[288,512]{1,0:T(8,128)(2,1)S(1)} collective-permute-done((bf16[288,512]{1,0:T(8,128)(2,1)S(1)}, bf16[288,512]{1,0:T(8,128)(2,1)S(1)}, u32[]{:S(2)}, u32[]{:S(2)}) %collective-permute-start.19) | collective-permute-done | bytes 294944 | tf_op jit(solution)/shard_map/ppermute | solution.py:95
  64.0 2.5 %collective-permute-start.9 = (f32[8,128]{1,0:T(8,128)S(1)}, f32[8,128]{1,0:T(8,128)S(1)}, u32[]{:S(2)}, u32[]{:S(2)}) collective-permute-start(f32[8,128]{1,0:T(8,128)S(1)} %shard_map.200.refs_2_), channel_id=1, source_target_pairs={{0,3},{1,2},{2,1},{3,0},{4,7},{5,6},{6,5},{7,4},{8,11},{9,10},{10,... | collective-permute-start | bytes 12296 | tf_op jit(solution)/shard_map/ppermute | solution.py:95
  67.5 1.0 %collective-permute-done.9.refs_5_ = f32[8,128]{1,0:T(8,128)S(1)} collective-permute-done((f32[8,128]{1,0:T(8,128)S(1)}, f32[8,128]{1,0:T(8,128)S(1)}, u32[]{:S(2)}, u32[]{:S(2)}) %collective-permute-start.9) | collective-permute-done | bytes 4128 | tf_op jit(solution)/shard_map/ppermute | solution.py:95
  68.5 1.6 %collective-permute-done.8.refs_4_ = f32[8,128]{1,0:T(8,128)S(1)} collective-permute-done((f32[8,128]{1,0:T(8,128)S(1)}, f32[8,128]{1,0:T(8,128)S(1)}, u32[]{:S(2)}, u32[]{:S(2)}) %collective-permute-start.8) | collective-permute-done | bytes 4128 | tf_op jit(solution)/shard_map/ppermute | solution.py:95
  70.7 5.1 %shard_map.201 = (f32[16,512]{1,0:T(8,128)}, f32[16,512]{1,0:T(8,128)}, f32[16,512]{1,0:T(8,128)}, f32[16,512]{1,0:T(8,128)}, f32[256,512]{1,0:T(8,128)}, /*inde...) custom-call(f32[128,512]{1,0:T(8,128)S(1)} %shard_map.199.a.refs_0_,, ...), custom_call_target="tpu_custom_call" | custom-call | tf_op jit(solution)/shard_map/pallas_call | solution.py:127
  (53 shorter events, 5.7 us)
Async XLA Ops:
  5.4 3.1 %collective-permute-start = (f32[128,2048]{1,0:T(8,128)}, f32[128,2048]{1,0:T(8,128)S(1)}, u32[]{:S(2)}, u32[]{:S(2)}) collective-permute-start(f32[128,2048]{1,0:T(8,128)} %get-tuple-element.19), channel_id=1, source_target_pairs={{0,4},{1,5},{2,6},{3,7},{4,0},{5,1},{6,2},{7,3},{8,12},{9,13},{10,... | collective-permute-start | bytes 3145736 | tf_op jit(solution)/shard_map/ppermute | solution.py:95
  10.4 8.5 %collective-permute-start.1 = (bf16[136,512]{1,0:T(8,128)(2,1)S(1)}, bf16[136,512]{1,0:T(8,128)(2,1)S(1)}, u32[]{:S(2)}, u32[]{:S(2)}) collective-permute-start(bf16[136,512]{1,0:T(8,128)(2,1)S(1)} %get-tuple-element.21), channel_id=1, source_target_pairs={{0,1},{1,0},{2,3},{3,2},{4,5},{5,4},{6,7},{7,6},{8,9},{9,8},{10,11... | collective-permute-start | bytes 417800 | tf_op jit(solution)/shard_map/ppermute | solution.py:95
  13.3 8.4 %collective-permute-start.2 = (bf16[136,512]{1,0:T(8,128)(2,1)S(1)}, bf16[136,512]{1,0:T(8,128)(2,1)S(1)}, u32[]{:S(2)}, u32[]{:S(2)}) collective-permute-start(bf16[136,512]{1,0:T(8,128)(2,1)S(1)} %get-tuple-element.22), channel_id=1, source_target_pairs={{0,2},{1,3},{2,0},{3,1},{4,6},{5,7},{6,4},{7,5},{8,10},{9,11},{10,... | collective-permute-start | bytes 417800 | tf_op jit(solution)/shard_map/ppermute | solution.py:95
  14.8 6.9 %collective-permute-start.3 = (bf16[136,512]{1,0:T(8,128)(2,1)S(1)}, bf16[136,512]{1,0:T(8,128)(2,1)S(1)}, u32[]{:S(2)}, u32[]{:S(2)}) collective-permute-start(bf16[136,512]{1,0:T(8,128)(2,1)S(1)} %get-tuple-element.23), channel_id=1, source_target_pairs={{0,3},{1,2},{2,1},{3,0},{4,7},{5,6},{6,5},{7,4},{8,11},{9,10},{10,... | collective-permute-start | bytes 417800 | tf_op jit(solution)/shard_map/ppermute | solution.py:95
  14.9 17.6 %collective-permute-start.16 = (bf16[288,512]{1,0:T(8,128)(2,1)}, bf16[288,512]{1,0:T(8,128)(2,1)S(1)}, u32[]{:S(2)}, u32[]{:S(2)}) collective-permute-start(bf16[288,512]{1,0:T(8,128)(2,1)} %get-tuple-element.24.refs_14_), channel_id=1, source_target_pairs={{0,24},{1,25},{2,26},{3,27},{4,28},{5,29},{6,30},{7,31},{8,16},{9,... | collective-permute-start | bytes 884744 | tf_op jit(solution)/shard_map/ppermute | solution.py:95
  22.3 7.2 %collective-permute-start.4 = (bf16[136,512]{1,0:T(8,128)(2,1)S(1)}, bf16[136,512]{1,0:T(8,128)(2,1)S(1)}, u32[]{:S(2)}, u32[]{:S(2)}) collective-permute-start(bf16[136,512]{1,0:T(8,128)(2,1)S(1)} %shard_map.197.a), channel_id=1, source_target_pairs={{0,8},{1,9},{2,10},{3,11},{4,12},{5,13},{6,14},{7,15},{8,0},{9,1},... | collective-permute-start | bytes 417800 | tf_op jit(solution)/shard_map/ppermute | solution.py:95
  23.9 13.0 %collective-permute-start.12 = (bf16[288,512]{1,0:T(8,128)(2,1)S(1)}, bf16[288,512]{1,0:T(8,128)(2,1)S(1)}, u32[]{:S(2)}, u32[]{:S(2)}) collective-permute-start(bf16[288,512]{1,0:T(8,128)(2,1)S(1)} %copy-done.5), channel_id=1, source_target_pairs={{0,8},{1,9},{2,10},{3,11},{4,12},{5,13},{6,14},{7,15},{8,0},{9,1},... | collective-permute-start | bytes 884744 | tf_op jit(solution)/shard_map/ppermute | solution.py:95
  24.4 12.6 %collective-permute-start.10 = (bf16[288,512]{1,0:T(8,128)(2,1)S(1)}, bf16[288,512]{1,0:T(8,128)(2,1)S(1)}, u32[]{:S(2)}, u32[]{:S(2)}) collective-permute-start(bf16[288,512]{1,0:T(8,128)(2,1)S(1)} %copy-done.5), channel_id=1, source_target_pairs={{0,4},{1,5},{2,6},{3,7},{4,0},{5,1},{6,2},{7,3},{8,12},{9,13},{10,... | collective-permute-start | bytes 884744 | tf_op jit(solution)/shard_map/ppermute | solution.py:95
  24.4 19.2 %collective-permute-start.18 = (bf16[288,512]{1,0:T(8,128)(2,1)S(1)}, bf16[288,512]{1,0:T(8,128)(2,1)S(1)}, u32[]{:S(2)}, u32[]{:S(2)}) collective-permute-start(bf16[288,512]{1,0:T(8,128)(2,1)S(1)} %copy-done.6), channel_id=1, source_target_pairs={{0,24},{1,25},{2,26},{3,27},{4,28},{5,29},{6,30},{7,31},{8,16},{9,... | collective-permute-start | bytes 884744 | tf_op jit(solution)/shard_map/ppermute | solution.py:95
  29.5 24.2 %collective-permute-start.13 = (bf16[288,512]{1,0:T(8,128)(2,1)S(1)}, bf16[288,512]{1,0:T(8,128)(2,1)S(1)}, u32[]{:S(2)}, u32[]{:S(2)}) collective-permute-start(bf16[288,512]{1,0:T(8,128)(2,1)S(1)} %copy-done.6), channel_id=1, source_target_pairs={{0,8},{1,9},{2,10},{3,11},{4,12},{5,13},{6,14},{7,15},{8,0},{9,1},... | collective-permute-start | bytes 884744 | tf_op jit(solution)/shard_map/ppermute | solution.py:95
  32.4 19.0 %collective-permute-start.5 = (bf16[136,512]{1,0:T(8,128)(2,1)S(1)}, bf16[136,512]{1,0:T(8,128)(2,1)S(1)}, u32[]{:S(2)}, u32[]{:S(2)}) collective-permute-start(bf16[136,512]{1,0:T(8,128)(2,1)S(1)} %shard_map.198.a), channel_id=1, source_target_pairs={{0,16},{1,17},{2,18},{3,19},{4,20},{5,21},{6,22},{7,23},{8,24},{9,... | collective-permute-start | bytes 417800 | tf_op jit(solution)/shard_map/ppermute | solution.py:95
  36.9 16.8 %collective-permute-start.11 = (bf16[288,512]{1,0:T(8,128)(2,1)S(1)}, bf16[288,512]{1,0:T(8,128)(2,1)S(1)}, u32[]{:S(2)}, u32[]{:S(2)}) collective-permute-start(bf16[288,512]{1,0:T(8,128)(2,1)S(1)} %copy-done.6), channel_id=1, source_target_pairs={{0,4},{1,5},{2,6},{3,7},{4,0},{5,1},{6,2},{7,3},{8,12},{9,13},{10,... | collective-permute-start | bytes 884744 | tf_op jit(solution)/shard_map/ppermute | solution.py:95
  37.0 17.3 %collective-permute-start.22 = (bf16[288,512]{1,0:T(8,128)(2,1)S(1)}, bf16[288,512]{1,0:T(8,128)(2,1)S(1)}, u32[]{:S(2)}, u32[]{:S(2)}) collective-permute-start(bf16[288,512]{1,0:T(8,128)(2,1)S(1)} %collective-permute-done.16.refs_26_), channel_id=1, source_target_pairs={{0,4},{1,5},{2,6},{3,7},{4,0},{5,1},{6,2},{7,3},{8,12},{9,13},{10,... | collective-permute-start | bytes 884744 | tf_op jit(solution)/shard_map/ppermute | solution.py:95
  43.6 14.2 %collective-permute-start.17 = (bf16[288,512]{1,0:T(8,128)(2,1)S(1)}, bf16[288,512]{1,0:T(8,128)(2,1)S(1)}, u32[]{:S(2)}, u32[]{:S(2)}) collective-permute-start(bf16[288,512]{1,0:T(8,128)(2,1)S(1)} %collective-permute-done.16.refs_26_), channel_id=1, source_target_pairs={{0,8},{1,9},{2,10},{3,11},{4,12},{5,13},{6,14},{7,15},{8,0},{9,1},... | collective-permute-start | bytes 884744 | tf_op jit(solution)/shard_map/ppermute | solution.py:95
  51.5 11.8 %collective-permute-start.19 = (bf16[288,512]{1,0:T(8,128)(2,1)S(1)}, bf16[288,512]{1,0:T(8,128)(2,1)S(1)}, u32[]{:S(2)}, u32[]{:S(2)}) collective-permute-start(bf16[288,512]{1,0:T(8,128)(2,1)S(1)} %collective-permute-done.18.refs_27_), channel_id=1, source_target_pairs={{0,8},{1,9},{2,10},{3,11},{4,12},{5,13},{6,14},{7,15},{8,0},{9,1},... | collective-permute-start | bytes 884744 | tf_op jit(solution)/shard_map/ppermute | solution.py:95
  53.7 9.5 %collective-permute-start.6 = (f32[128,512]{1,0:T(8,128)S(1)}, f32[128,512]{1,0:T(8,128)S(1)}, u32[]{:S(2)}, u32[]{:S(2)}) collective-permute-start(f32[128,512]{1,0:T(8,128)S(1)} %shard_map.199.a.refs_0_), channel_id=1, source_target_pairs={{0,4},{1,5},{2,6},{3,7},{4,0},{5,1},{6,2},{7,3},{8,12},{9,13},{10,... | collective-permute-start | bytes 786440 | tf_op jit(solution)/shard_map/ppermute | solution.py:95
  53.8 10.2 %collective-permute-start.14 = (bf16[288,512]{1,0:T(8,128)(2,1)S(1)}, bf16[288,512]{1,0:T(8,128)(2,1)S(1)}, u32[]{:S(2)}, u32[]{:S(2)}) collective-permute-start(bf16[288,512]{1,0:T(8,128)(2,1)S(1)} %collective-permute-done.12.refs_18_), channel_id=1, source_target_pairs={{0,4},{1,5},{2,6},{3,7},{4,0},{5,1},{6,2},{7,3},{8,12},{9,13},{10,... | collective-permute-start | bytes 884744 | tf_op jit(solution)/shard_map/ppermute | solution.py:95
  54.3 12.2 %collective-permute-start.23 = (bf16[288,512]{1,0:T(8,128)(2,1)S(1)}, bf16[288,512]{1,0:T(8,128)(2,1)S(1)}, u32[]{:S(2)}, u32[]{:S(2)}) collective-permute-start(bf16[288,512]{1,0:T(8,128)(2,1)S(1)} %collective-permute-done.18.refs_27_), channel_id=1, source_target_pairs={{0,4},{1,5},{2,6},{3,7},{4,0},{5,1},{6,2},{7,3},{8,12},{9,13},{10,... | collective-permute-start | bytes 884744 | tf_op jit(solution)/shard_map/ppermute | solution.py:95
  57.8 9.2 %collective-permute-start.15 = (bf16[288,512]{1,0:T(8,128)(2,1)S(1)}, bf16[288,512]{1,0:T(8,128)(2,1)S(1)}, u32[]{:S(2)}, u32[]{:S(2)}) collective-permute-start(bf16[288,512]{1,0:T(8,128)(2,1)S(1)} %collective-permute-done.13.refs_19_), channel_id=1, source_target_pairs={{0,4},{1,5},{2,6},{3,7},{4,0},{5,1},{6,2},{7,3},{8,12},{9,13},{10,... | collective-permute-start | bytes 884744 | tf_op jit(solution)/shard_map/ppermute | solution.py:95
  63.2 4.3 %collective-permute-start.20 = (bf16[288,512]{1,0:T(8,128)(2,1)S(1)}, bf16[288,512]{1,0:T(8,128)(2,1)S(1)}, u32[]{:S(2)}, u32[]{:S(2)}) collective-permute-start(bf16[288,512]{1,0:T(8,128)(2,1)S(1)} %collective-permute-done.17.refs_22_), channel_id=1, source_target_pairs={{0,4},{1,5},{2,6},{3,7},{4,0},{5,1},{6,2},{7,3},{8,12},{9,13},{10,... | collective-permute-start | bytes 884744 | tf_op jit(solution)/shard_map/ppermute | solution.py:95
  63.3 4.3 %collective-permute-start.21 = (bf16[288,512]{1,0:T(8,128)(2,1)S(1)}, bf16[288,512]{1,0:T(8,128)(2,1)S(1)}, u32[]{:S(2)}, u32[]{:S(2)}) collective-permute-start(bf16[288,512]{1,0:T(8,128)(2,1)S(1)} %collective-permute-done.19.refs_23_), channel_id=1, source_target_pairs={{0,4},{1,5},{2,6},{3,7},{4,0},{5,1},{6,2},{7,3},{8,12},{9,13},{10,... | collective-permute-start | bytes 884744 | tf_op jit(solution)/shard_map/ppermute | solution.py:95
  64.0 4.6 %collective-permute-start.9 = (f32[8,128]{1,0:T(8,128)S(1)}, f32[8,128]{1,0:T(8,128)S(1)}, u32[]{:S(2)}, u32[]{:S(2)}) collective-permute-start(f32[8,128]{1,0:T(8,128)S(1)} %shard_map.200.refs_2_), channel_id=1, source_target_pairs={{0,3},{1,2},{2,1},{3,0},{4,7},{5,6},{6,5},{7,4},{8,11},{9,10},{10,... | collective-permute-start | bytes 12296 | tf_op jit(solution)/shard_map/ppermute | solution.py:95
  66.5 3.6 %collective-permute-start.8 = (f32[8,128]{1,0:T(8,128)S(1)}, f32[8,128]{1,0:T(8,128)S(1)}, u32[]{:S(2)}, u32[]{:S(2)}) collective-permute-start(f32[8,128]{1,0:T(8,128)S(1)} %shard_map.200.refs_2_), channel_id=1, source_target_pairs={{0,2},{1,3},{2,0},{3,1},{4,6},{5,7},{6,4},{7,5},{8,10},{9,11},{10,... | collective-permute-start | bytes 12296 | tf_op jit(solution)/shard_map/ppermute | solution.py:95
  67.0 3.6 %collective-permute-start.7 = (f32[8,128]{1,0:T(8,128)S(1)}, f32[8,128]{1,0:T(8,128)S(1)}, u32[]{:S(2)}, u32[]{:S(2)}) collective-permute-start(f32[8,128]{1,0:T(8,128)S(1)} %shard_map.200.refs_2_), channel_id=1, source_target_pairs={{0,1},{1,0},{2,3},{3,2},{4,5},{5,4},{6,7},{7,6},{8,9},{9,8},{10,11... | collective-permute-start | bytes 12296 | tf_op jit(solution)/shard_map/ppermute | solution.py:95
  (11 other events, 517.2 us)

commit v2 on v1

--- a/solution.py
+++ b/solution.py
@@ -99,6 +99,8 @@
 VMEM = pl.BlockSpec(memory_space=pltpu.VMEM)
 HBM = pl.BlockSpec(memory_space=pltpu.HBM)
 TAG = 8
+PIECES = 2
+CUTS = (3,)
 
 
 def shape(*dims, dtype=jnp.float32):
@@ -134,17 +136,52 @@
     )(*args)
 
 
-def begin(stored, saved, cotangents, bases):
+def in_hbm(arrays):
+    return [pltpu.with_memory_space_constraint(a, pltpu.HBM) for a in arrays]
+
+
+def pack(stored, cuts):
+    cols = stored[0].shape[1]
+    packed = sum(a.shape[0] for a in stored)
+    count = len(stored)
+    edges = [0, *cuts, packed]
+
+    def kernel(*refs):
+        sources, outs = refs[:count], refs[count : count + len(edges)]
+        held, sems = refs[count + len(edges) : -1], refs[-1]
+        copies = [
+            pltpu.make_async_copy(src, dst, sems.at[n])
+            for n, (src, dst) in enumerate(zip(sources, held))
+        ]
+        for copy in copies:
+            copy.start()
+        row = 0
+        for n in range(count):
+            copies[n].wait()
+            size = held[n].shape[0]
+            value = code(held[n][...] * (1.0 / PLAIN_UNIT))
+            outs[0][row : row + size, :] = value
+            for part, low, high in zip(outs[1:], edges, edges[1:]):
+                first, last = max(low, row), min(high, row + size)
+                if first < last:
+                    part[first - low : last - low, :] = value[first - row : last - row, :]
+            row += size
+
+    scratch = [pltpu.VMEM(a.shape, a.dtype) for a in stored]
+    scratch += [pltpu.SemaphoreType.DMA((count,))]
+    sizes = [packed] + [high - low for low, high in zip(edges, edges[1:])]
+    outs = [shape(n, cols, dtype=jnp.bfloat16) for n in sizes]
+    return call(kernel, outs, in_hbm(stored), 6, hbm_args=True, scratch=scratch)
+
+
+def low_terms(saved, cotangents, bases):
     rank, width = bases[0].shape[1], cotangents[0].shape[1]
-    cols = stored[0][0].shape[1]
-    packed = sum(a.shape[0] for a in stored[0])
-    first = len(stored[0])
-    arrays = (*stored[0], *stored[1], bases[0], saved[0], cotangents[0], bases[1], saved[1], cotangents[1])
+    arrays = (bases[0], saved[0], bases[1], saved[1], *cotangents)
     count = len(arrays)
 
     def kernel(*refs):
-        sources, outs = refs[:count], refs[count : count + 4]
-        held, sems = refs[count + 4 : 2 * count + 4], refs[2 * count + 4]
+        sources, (give, keep) = refs[:count], refs[count : count + 2]
+        held, sems = refs[count + 2 : 2 * count + 2], refs[2 * count + 2]
         core = lax.axis_index("fs") % CORES
         copies = [
             pltpu.make_async_copy(src, dst, sems.at[n])
@@ -152,39 +189,35 @@
         ]
         for copy in copies:
             copy.start()
+        reduced = []
         for which in range(2):
-            row = 0
-            for n in range(which * first, (which + 1) * first):
-                copies[n].wait()
-                size = held[n].shape[0]
-                outs[which][row : row + size, :] = code(held[n][...] * (1.0 / PLAIN_UNIT))
-                row += size
+            copies[2 * which].wait()
+            copies[2 * which + 1].wait()
+            value = jnp.dot(
+                held[2 * which + 1][...], held[2 * which][...], preferred_element_type=jnp.float32
+            )
+            reduced.append(value.astype(jnp.bfloat16))
         for which in range(2):
-            at = 2 * first + 3 * which
-            copies[at].wait()
-            copies[at + 1].wait()
-            reduced = jnp.dot(
-                held[at + 1][...], held[at][...], preferred_element_type=jnp.float32
-            )
-            copies[at + 2].wait()
+            copies[4 + which].wait()
             term = lax.dot_general(
-                reduced.astype(jnp.bfloat16),
-                held[at + 2][...],
+                reduced[which],
+                held[4 + which][...],
                 (((0,), (0,)), ((), ())),
                 preferred_element_type=jnp.float32,
             )
 
             @pl.when(core == which)
             def _():
-                outs[3][...] = term
+                keep[...] = term
 
             @pl.when(core != which)
             def _():
-                outs[2][...] = term
-
-    scratch = [pltpu.VMEM(a.shape, a.dtype) for a in arrays] + [pltpu.SemaphoreType.DMA((count,))]
-    outs = [shape(packed, cols, dtype=jnp.bfloat16)] * 2 + [shape(rank, width)] * 2
-    return call(kernel, outs, arrays, 60, hbm_args=True, scratch=scratch)
+                give[...] = term
+
+    scratch = [pltpu.VMEM(a.shape, a.dtype) for a in arrays]
+    scratch += [pltpu.SemaphoreType.DMA((count,))]
+    outs = [shape(rank, width)] * 2
+    return call(kernel, outs, in_hbm(arrays), 12, hbm_args=True, scratch=scratch)
 
 
 def put_coded(ref, value, unit):
@@ -255,6 +288,8 @@
     full, rank = bases[0].shape
     here = old[0].shape[0]
     n_sq, n_bl = len(squares), len(blocks)
+    piece = rows // PIECES
+    flat = [a for block in blocks for a in block]
 
     def kernel(*refs):
         refs = list(refs)
@@ -269,7 +304,7 @@
         basis_refs = take(2)
         master_refs = take(2)
         old_refs = take(4)
-        block_refs = [take(2) for _ in range(n_bl)]
+        block_refs = [take(len(block)) for block in blocks]
         outs = take(10)
         grads, direction, small, own, stage, sems = refs
         me = lax.axis_index("fs")
@@ -279,6 +314,12 @@
         def send(src, dst):
             copies.append(pltpu.make_async_copy(src, dst, sems.at[len(copies)]))
             copies[-1].start()
+
+        def packed(n, row, size):
+            for ref in block_refs[n]:
+                if row < ref.shape[0]:
+                    return uncode(ref[row : row + size, :]) * PLAIN_UNIT
+                row -= ref.shape[0]
 
         squares = square_refs[0][...]
         for ref in square_refs[1:]:
@@ -289,44 +330,44 @@
         grads[0] = jnp.where(core == 0, mine, theirs)
         grads[1] = jnp.where(core == 0, theirs, mine)
         for which in range(2):
-            grad = grads[which, pl.ds(pl.multiple_of(me * here, here), here), :]
-            new = moments(old_refs[2 * which][...], old_refs[2 * which + 1][...], grad)
-            for j in range(2):
-                small[2 * which + j] = new[j]
-                send(small.at[2 * which + j], outs[2 * which + j])
-        for n in range(n_bl):
-            at = pl.multiple_of((me ^ n) * here, here)
-            for which in range(2):
-                ref = block_refs[n][which]
-                first = uncode(ref[rows : rows + here, :]) * PLAIN_UNIT
-                second = uncode(ref[rows + here : rows + 2 * here, :]) * PLAIN_UNIT
+            for n in range(n_bl):
+                at = pl.multiple_of((me ^ n) * here, here)
+                first = packed(n, 2 * which * here, here)
+                second = packed(n, (2 * which + 1) * here, here)
                 value = moments(first, second, grads[which, pl.ds(at, here), :])[2]
                 high = value.astype(jnp.bfloat16)
                 direction[which, pl.ds(at, here), :] = high
                 direction[which, pl.ds(pl.multiple_of(rank + at, here), here), :] = (
                     value - high.astype(jnp.float32)
                 ).astype(jnp.bfloat16)
-
-        for n in range(n_bl):
-            row0 = pl.multiple_of((me ^ n) * rows, rows)
-            for which in range(2):
-                b = basis_refs[which][pl.ds(row0, rows), :]
-                both = jnp.concatenate([b, b], axis=1)
-                down = jnp.dot(both, direction[which], preferred_element_type=jnp.float32)
+            for n in range(n_bl):
+                for p in range(PIECES):
+                    row0 = pl.multiple_of((me ^ n) * rows + p * piece, piece)
+                    b = basis_refs[which][pl.ds(row0, piece), :]
+                    both = jnp.concatenate([b, b], axis=1)
+                    down = jnp.dot(both, direction[which], preferred_element_type=jnp.float32)
+                    at = slice(p * piece, (p + 1) * piece)
+                    if n == 0:
+                        own[which, at, :] = -down
+                        own[2 + which, at, :] = master_refs[which][at, :] - down
+                    value = packed(n, 4 * here + which * rows + p * piece, piece)
+                    stage[2 * n + which, at, :] = (value - down).astype(jnp.bfloat16)
                 if n == 0:
-                    own[which] = -down
-                    own[2 + which] = master_refs[which][...] - down
                     for j in (which, 2 + which):
                         send(own.at[j], outs[4 + j])
-                value = uncode(block_refs[n][which][:rows, :]) * PLAIN_UNIT
-                stage[2 * n + which] = (value - down).astype(jnp.bfloat16)
+                row0 = pl.multiple_of((me ^ n) * rows, rows)
                 send(stage.at[2 * n + which], outs[8 + which].at[pl.ds(row0, rows), :])
+        for which in range(2):
+            grad = grads[which, pl.ds(pl.multiple_of(me * here, here), here), :]
+            new = moments(old_refs[2 * which][...], old_refs[2 * which + 1][...], grad)
+            for j in range(2):
+                small[2 * which + j] = new[j]
+                send(small.at[2 * which + j], outs[2 * which + j])
         for copy in copies:
             copy.wait()
 
     outs = [shape(here, cols)] * 4 + [shape(rows, cols)] * 4
     outs += [shape(full, cols, dtype=jnp.bfloat16)] * 2
-    flat = [array for block in blocks for array in block]
     args = (total, other, *squares, *bases, *masters, *old, *flat)
     scratch = [
         pltpu.VMEM((2, rank, cols), jnp.float32),
@@ -360,29 +401,30 @@
     old = (in_first, in_second, point_first, point_second)
     bases = (in_basis, point_basis)
 
-    *packs, give, keep = begin(
-        ((in_master, in_first, in_second), (point_master, point_first, point_second)),
-        (in_saved, point_saved),
-        (in_cotangent, point_cotangent),
-        bases,
+    piece = in_master.shape[0] // PIECES
+    at = [len(old) * in_first.shape[0] + n * piece for n in CUTS]
+    whole, *parts = pack((*old, *masters), at)
+    one = exchange(whole, CORES)
+    three = [exchange(p, 3 * CORES) for p in parts]
+
+    give, keep = low_terms(
+        (in_saved, point_saved), (in_cotangent, point_cotangent), bases
     )
     given = exchange(give, 1)
-    one = [exchange(p, CORES) for p in packs]
-    three = [exchange(p, 3 * CORES) for p in packs]
-
     mine, *coded = chip_sum(keep, given, tp_count)
     got = [exchange(coded[k - 1], 0, k) for k in range(1, tp_count)]
     coded = plane_sum(mine, got)
     coded = pair_sum(coded, exchange(coded, CORES), False)
     total = pair_sum(coded, exchange(coded, 2 * CORES), True)
     two = [exchange(t, CORES) for t in three]
+
     other = exchange(total, 1)
     squares = square_sum(total, other)
     squares = [squares] + [exchange(squares, 0, k) for k in range(1, tp_count)]
-    blocks = []
-    for arrays in (packs, one, two, three):
-        swapped = [exchange(a, 1) for a in arrays]
-        blocks += [arrays, swapped]
+
+    blocks = [[whole], [exchange(whole, 1)], [one], [exchange(one, 1)]]
+    for arrays in (two, three):
+        blocks += [arrays, [exchange(a, 1) for a in arrays]]
     return tuple(finish(entries, total, other, squares, bases, masters, old, blocks))
 
 

time: 75.9 us -> 75.2 us (level)
  local copies, waits for them, and re-layouts: 1.28 us -> 0.05 us
  starting transfers between devices: 27.9 us -> 28.8 us
    unnamed x22 -> x16, local copies, waits for them, and re-layouts: 1.28 us -> 0.05 us
    ppermute x24 -> x21, starting transfers between devices: 27.9 us -> 28.8 us  [exchange(): return lax.ppermute(x, ('fs', 'tp'), pairs)]
    pallas_call x7 -> x8, Pallas kernels: 11.8 us -> 11.4 us  [call(): pl.pallas_call(kernel, out_shape=outs, in_specs=[HBM if hbm_args else VME...]
    ppermute x24 -> x21, waiting for transfers between devices: 33.9 us -> 34 us  [exchange(): return lax.ppermute(x, ('fs', 'tp'), pairs)]
  transfers between devices with their start and end apart: 24 -> 21, of which waited for: 11 -> 10; matrix products, arithmetic and copies ran while one was open for 0% -> 0% of each run, Pallas kernels for 2% -> 5%
where the time goes in v2:
time: 75.2 us; the launch traced here: 75 us
  waiting for transfers between devices  34 us (45%)
  starting transfers between devices  28.8 us (38%)
  Pallas kernels  11.4 us (15%)
  between operations  0.82 us (1%)
    ppermute x21, waiting for transfers between devices, exchange(): return lax.ppermute(x, ('fs', 'tp'), pairs)  34 us
    ppermute x21, starting transfers between devices, exchange(): return lax.ppermute(x, ('fs', 'tp'), pairs)  28.8 us
    pallas_call x8, Pallas kernels, call(): pl.pallas_call(kernel, out_shape=outs, in_specs=[HBM if hbm_args else VME...  11.4 us
  transfers between devices with their start and end apart: 21, of which 10 were waited for; matrix products, arithmetic and copies ran while one was open for 0% of the time, Pallas kernels for 5%

profile of v2, /device:TPU:0, one launch (start us, length us, event | category | flops | bytes accessed | tf_op | source)
XLA Modules:
  0.0 75.0 jit_solution(2653415772053881150)
XLA Ops:
  0.6 2.9 %shard_map.195 = (f32[128,2048]{1,0:T(8,128)S(1)}, f32[128,2048]{1,0:T(8,128)S(1)}) custom-call(bf16[2048,128]{1,0:T(8,128)(2,1)} %refs_6_.1, bf16[192,2048]{1,0:T(8,128)(2,1)} %refs_1_.2, bf16[2048,128]{1,0:T(8,128)(2,1)} %refs_7_.1, bf16[192,2048]{1,0:T(8,128)(2,1)} %refs_3_.2, bf16[192,2048]{1,0:T(8,128)(2,1)} %refs_4_.2, bf16[192,2048]{1,0:T(8,128)(2,1)} %refs_5_.2), custom_call_target="tpu_custom_call" | custom-call | tf_op jit(solution)/shard_map/pallas_call | solution.py:129
  3.5 0.6 collective-permute-start
  4.1 1.5 %shard_map.201 = (bf16[576,512]{1,0:T(8,128)(2,1)S(1)}, bf16[448,512]{1,0:T(8,128)(2,1)S(1)}, bf16[128,512]{1,0:T(8,128)(2,1)S(1)}) custom-call(f32[16,512]{1,0:T(8,128)} %refs_10_.1, f32[16,512]{1,0:T(8,128)} %refs_11_.1, f32[16,512]{1,0:T(8,128)} %refs_12_.1, f32[16,512]{1,0:T(8,128)} %refs_13_.1, f32[256,512]{1,0:T(8,128)} %refs_8_.1, f32[256,512]{1,0:T(8,128)} %refs_9_.1), custom_call_target="tpu_custom_call" | custom-call | tf_op jit(solution)/shard_map/pallas_call | solution.py:129
  5.5 4.7 %collective-permute-start.13 = (bf16[448,512]{1,0:T(8,128)(2,1)S(1)}, bf16[448,512]{1,0:T(8,128)(2,1)S(1)}, u32[]{:S(2)}, u32[]{:S(2)}) collective-permute-start(bf16[448,512]{1,0:T(8,128)(2,1)S(1)} %get-tuple-element.26), channel_id=1, source_target_pairs={{0,24},{1,25},{2,26},{3,27},{4,28},{5,29},{6,30},{7,31},{8,16},{9,... | collective-permute-start | bytes 1376264 | tf_op jit(solution)/shard_map/ppermute | solution.py:95
  10.3 0.6 shard_map.196
  10.9 1.6 %collective-permute-start.1 = (bf16[136,512]{1,0:T(8,128)(2,1)S(1)}, bf16[136,512]{1,0:T(8,128)(2,1)S(1)}, u32[]{:S(2)}, u32[]{:S(2)}) collective-permute-start(bf16[136,512]{1,0:T(8,128)(2,1)S(1)} %get-tuple-element.22), channel_id=1, source_target_pairs={{0,1},{1,0},{2,3},{3,2},{4,5},{5,4},{6,7},{7,6},{8,9},{9,8},{10,11... | collective-permute-start | bytes 417800 | tf_op jit(solution)/shard_map/ppermute | solution.py:95
  12.4 9.2 %collective-permute-done.13.refs_22_ = bf16[448,512]{1,0:T(8,128)(2,1)S(1)} collective-permute-done((bf16[448,512]{1,0:T(8,128)(2,1)S(1)}, bf16[448,512]{1,0:T(8,128)(2,1)S(1)}, u32[]{:S(2)}, u32[]{:S(2)}) %collective-permute-start.13) | collective-permute-done | bytes 458784 | tf_op jit(solution)/shard_map/ppermute | solution.py:95
  21.7 9.3 %collective-permute-start.14 = (bf16[448,512]{1,0:T(8,128)(2,1)S(1)}, bf16[448,512]{1,0:T(8,128)(2,1)S(1)}, u32[]{:S(2)}, u32[]{:S(2)}) collective-permute-start(bf16[448,512]{1,0:T(8,128)(2,1)S(1)} %collective-permute-done.13.refs_22_), channel_id=1, source_target_pairs={{0,8},{1,9},{2,10},{3,11},{4,12},{5,13},{6,14},{7,15},{8,0},{9,1},... | collective-permute-start | bytes 1376264 | tf_op jit(solution)/shard_map/ppermute | solution.py:95
  30.9 1.5 %collective-permute-start.2 = (bf16[136,512]{1,0:T(8,128)(2,1)S(1)}, bf16[136,512]{1,0:T(8,128)(2,1)S(1)}, u32[]{:S(2)}, u32[]{:S(2)}) collective-permute-start(bf16[136,512]{1,0:T(8,128)(2,1)S(1)} %get-tuple-element.23), channel_id=1, source_target_pairs={{0,2},{1,3},{2,0},{3,1},{4,6},{5,7},{6,4},{7,5},{8,10},{9,11},{10,... | collective-permute-start | bytes 417800 | tf_op jit(solution)/shard_map/ppermute | solution.py:95
  32.4 1.4 %collective-permute-start.3 = (bf16[136,512]{1,0:T(8,128)(2,1)S(1)}, bf16[136,512]{1,0:T(8,128)(2,1)S(1)}, u32[]{:S(2)}, u32[]{:S(2)}) collective-permute-start(bf16[136,512]{1,0:T(8,128)(2,1)S(1)} %get-tuple-element.24), channel_id=1, source_target_pairs={{0,3},{1,2},{2,1},{3,0},{4,7},{5,6},{6,5},{7,4},{8,11},{9,10},{10,... | collective-permute-start | bytes 417800 | tf_op jit(solution)/shard_map/ppermute | solution.py:95
  33.9 2.5 %collective-permute-start.15 = (bf16[128,512]{1,0:T(8,128)(2,1)S(1)}, bf16[128,512]{1,0:T(8,128)(2,1)S(1)}, u32[]{:S(2)}, u32[]{:S(2)}) collective-permute-start(bf16[128,512]{1,0:T(8,128)(2,1)S(1)} %get-tuple-element.27), channel_id=1, source_target_pairs={{0,24},{1,25},{2,26},{3,27},{4,28},{5,29},{6,30},{7,31},{8,16},{9,... | collective-permute-start | bytes 393224 | tf_op jit(solution)/shard_map/ppermute | solution.py:95
  36.4 2.6 %collective-permute-done.2.refs_1_ = bf16[136,512]{1,0:T(8,128)(2,1)S(1)} collective-permute-done((bf16[136,512]{1,0:T(8,128)(2,1)S(1)}, bf16[136,512]{1,0:T(8,128)(2,1)S(1)}, u32[]{:S(2)}, u32[]{:S(2)}) %collective-permute-start.2) | collective-permute-done | bytes 139296 | tf_op jit(solution)/shard_map/ppermute | solution.py:95
  39.7 7.8 %collective-permute-done.15.refs_23_ = bf16[128,512]{1,0:T(8,128)(2,1)S(1)} collective-permute-done((bf16[128,512]{1,0:T(8,128)(2,1)S(1)}, bf16[128,512]{1,0:T(8,128)(2,1)S(1)}, u32[]{:S(2)}, u32[]{:S(2)}) %collective-permute-start.15) | collective-permute-done | bytes 131104 | tf_op jit(solution)/shard_map/ppermute | solution.py:95
  47.6 2.2 %collective-permute-done.4.b = bf16[136,512]{1,0:T(8,128)(2,1)S(1)} collective-permute-done((bf16[136,512]{1,0:T(8,128)(2,1)S(1)}, bf16[136,512]{1,0:T(8,128)(2,1)S(1)}, u32[]{:S(2)}, u32[]{:S(2)}) %collective-permute-start.4) | collective-permute-done | bytes 139296 | tf_op jit(solution)/shard_map/ppermute | solution.py:95
  50.2 0.6 collective-permute-start.5
  51.3 1.7 %collective-permute-start.16 = (bf16[128,512]{1,0:T(8,128)(2,1)S(1)}, bf16[128,512]{1,0:T(8,128)(2,1)S(1)}, u32[]{:S(2)}, u32[]{:S(2)}) collective-permute-start(bf16[128,512]{1,0:T(8,128)(2,1)S(1)} %collective-permute-done.15.refs_23_), channel_id=1, source_target_pairs={{0,8},{1,9},{2,10},{3,11},{4,12},{5,13},{6,14},{7,15},{8,0},{9,1},... | collective-permute-start | bytes 393224 | tf_op jit(solution)/shard_map/ppermute | solution.py:95
  53.1 6.7 %collective-permute-done.5.b = bf16[136,512]{1,0:T(8,128)(2,1)S(1)} collective-permute-done((bf16[136,512]{1,0:T(8,128)(2,1)S(1)}, bf16[136,512]{1,0:T(8,128)(2,1)S(1)}, u32[]{:S(2)}, u32[]{:S(2)}) %collective-permute-start.5) | collective-permute-done | bytes 139296 | tf_op jit(solution)/shard_map/ppermute | solution.py:95
  60.0 0.6 collective-permute-start.6
  60.6 1.4 %collective-permute-done.6.b.refs_1_ = f32[128,512]{1,0:T(8,128)S(1)} collective-permute-done((f32[128,512]{1,0:T(8,128)S(1)}, f32[128,512]{1,0:T(8,128)S(1)}, u32[]{:S(2)}, u32[]{:S(2)}) %collective-permute-start.6) | collective-permute-done | bytes 262176 | tf_op jit(solution)/shard_map/ppermute | solution.py:95
  62.3 1.0 %collective-permute-done.18.refs_21_ = bf16[128,512]{1,0:T(8,128)(2,1)S(1)} collective-permute-done((bf16[128,512]{1,0:T(8,128)(2,1)S(1)}, bf16[128,512]{1,0:T(8,128)(2,1)S(1)}, u32[]{:S(2)}, u32[]{:S(2)}) %collective-permute-start.18) | collective-permute-done | bytes 131104 | tf_op jit(solution)/shard_map/ppermute | solution.py:95
  63.3 2.5 %collective-permute-start.9 = (f32[8,128]{1,0:T(8,128)S(1)}, f32[8,128]{1,0:T(8,128)S(1)}, u32[]{:S(2)}, u32[]{:S(2)}) collective-permute-start(f32[8,128]{1,0:T(8,128)S(1)} %shard_map.200.refs_2_), channel_id=1, source_target_pairs={{0,3},{1,2},{2,1},{3,0},{4,7},{5,6},{6,5},{7,4},{8,11},{9,10},{10,... | collective-permute-start | bytes 12296 | tf_op jit(solution)/shard_map/ppermute | solution.py:95
  66.8 1.0 %collective-permute-done.9.refs_5_ = f32[8,128]{1,0:T(8,128)S(1)} collective-permute-done((f32[8,128]{1,0:T(8,128)S(1)}, f32[8,128]{1,0:T(8,128)S(1)}, u32[]{:S(2)}, u32[]{:S(2)}) %collective-permute-start.9) | collective-permute-done | bytes 4128 | tf_op jit(solution)/shard_map/ppermute | solution.py:95
  67.8 1.6 %collective-permute-done.8.refs_4_ = f32[8,128]{1,0:T(8,128)S(1)} collective-permute-done((f32[8,128]{1,0:T(8,128)S(1)}, f32[8,128]{1,0:T(8,128)S(1)}, u32[]{:S(2)}, u32[]{:S(2)}) %collective-permute-start.8) | collective-permute-done | bytes 4128 | tf_op jit(solution)/shard_map/ppermute | solution.py:95
  69.9 5.1 %shard_map.202 = (f32[16,512]{1,0:T(8,128)}, f32[16,512]{1,0:T(8,128)}, f32[16,512]{1,0:T(8,128)}, f32[16,512]{1,0:T(8,128)}, f32[256,512]{1,0:T(8,128)}, /*inde...) custom-call(f32[128,512]{1,0:T(8,128)S(1)} %shard_map.199.a.refs_0_,, ...), custom_call_target="tpu_custom_call" | custom-call | tf_op jit(solution)/shard_map/pallas_call | solution.py:129
  (42 shorter events, 3.9 us)
Async XLA Ops:
  3.5 6.7 %collective-permute-start = (f32[128,2048]{1,0:T(8,128)S(1)}, f32[128,2048]{1,0:T(8,128)S(1)}, u32[]{:S(2)}, u32[]{:S(2)}) collective-permute-start(f32[128,2048]{1,0:T(8,128)S(1)} %get-tuple-element.20), channel_id=1, source_target_pairs={{0,4},{1,5},{2,6},{3,7},{4,0},{5,1},{6,2},{7,3},{8,12},{9,13},{10,... | collective-permute-start | bytes 3145736 | tf_op jit(solution)/shard_map/ppermute | solution.py:95
  5.5 16.1 %collective-permute-start.13 = (bf16[448,512]{1,0:T(8,128)(2,1)S(1)}, bf16[448,512]{1,0:T(8,128)(2,1)S(1)}, u32[]{:S(2)}, u32[]{:S(2)}) collective-permute-start(bf16[448,512]{1,0:T(8,128)(2,1)S(1)} %get-tuple-element.26), channel_id=1, source_target_pairs={{0,24},{1,25},{2,26},{3,27},{4,28},{5,29},{6,30},{7,31},{8,16},{9,... | collective-permute-start | bytes 1376264 | tf_op jit(solution)/shard_map/ppermute | solution.py:95
  10.2 40.6 %collective-permute-start.11 = (bf16[576,512]{1,0:T(8,128)(2,1)S(1)}, bf16[576,512]{1,0:T(8,128)(2,1)S(1)}, u32[]{:S(2)}, u32[]{:S(2)}) collective-permute-start(bf16[576,512]{1,0:T(8,128)(2,1)S(1)} %get-tuple-element.25.refs_14_), channel_id=1, source_target_pairs={{0,8},{1,9},{2,10},{3,11},{4,12},{5,13},{6,14},{7,15},{8,0},{9,1},... | collective-permute-start | bytes 1769480 | tf_op jit(solution)/shard_map/ppermute | solution.py:95
  10.2 59.7 %copy-start = (f32[256,512]{1,0:T(8,128)S(1)}, f32[256,512]{1,0:T(8,128)}, u32[]{:S(2)}) copy-start(f32[256,512]{1,0:T(8,128)} %refs_8_.1) | copy-start | bytes 1572868
  10.2 59.7 %copy-start.1 = (f32[256,512]{1,0:T(8,128)S(1)}, f32[256,512]{1,0:T(8,128)}, u32[]{:S(2)}) copy-start(f32[256,512]{1,0:T(8,128)} %refs_9_.1) | copy-start | bytes 1572868
  10.2 59.7 %copy-start.2 = (bf16[2048,128]{1,0:T(8,128)(2,1)S(1)}, bf16[2048,128]{1,0:T(8,128)(2,1)}, u32[]{:S(2)}) copy-start(bf16[2048,128]{1,0:T(8,128)(2,1)} %refs_6_.1) | copy-start | bytes 1572868
  10.9 23.0 %collective-permute-start.1 = (bf16[136,512]{1,0:T(8,128)(2,1)S(1)}, bf16[136,512]{1,0:T(8,128)(2,1)S(1)}, u32[]{:S(2)}, u32[]{:S(2)}) collective-permute-start(bf16[136,512]{1,0:T(8,128)(2,1)S(1)} %get-tuple-element.22), channel_id=1, source_target_pairs={{0,1},{1,0},{2,3},{3,2},{4,5},{5,4},{6,7},{7,6},{8,9},{9,8},{10,11... | collective-permute-start | bytes 417800 | tf_op jit(solution)/shard_map/ppermute | solution.py:95
  21.7 31.4 %collective-permute-start.14 = (bf16[448,512]{1,0:T(8,128)(2,1)S(1)}, bf16[448,512]{1,0:T(8,128)(2,1)S(1)}, u32[]{:S(2)}, u32[]{:S(2)}) collective-permute-start(bf16[448,512]{1,0:T(8,128)(2,1)S(1)} %collective-permute-done.13.refs_22_), channel_id=1, source_target_pairs={{0,8},{1,9},{2,10},{3,11},{4,12},{5,13},{6,14},{7,15},{8,0},{9,1},... | collective-permute-start | bytes 1376264 | tf_op jit(solution)/shard_map/ppermute | solution.py:95
  30.9 8.0 %collective-permute-start.2 = (bf16[136,512]{1,0:T(8,128)(2,1)S(1)}, bf16[136,512]{1,0:T(8,128)(2,1)S(1)}, u32[]{:S(2)}, u32[]{:S(2)}) collective-permute-start(bf16[136,512]{1,0:T(8,128)(2,1)S(1)} %get-tuple-element.23), channel_id=1, source_target_pairs={{0,2},{1,3},{2,0},{3,1},{4,6},{5,7},{6,4},{7,5},{8,10},{9,11},{10,... | collective-permute-start | bytes 417800 | tf_op jit(solution)/shard_map/ppermute | solution.py:95
  32.4 6.5 %collective-permute-start.3 = (bf16[136,512]{1,0:T(8,128)(2,1)S(1)}, bf16[136,512]{1,0:T(8,128)(2,1)S(1)}, u32[]{:S(2)}, u32[]{:S(2)}) collective-permute-start(bf16[136,512]{1,0:T(8,128)(2,1)S(1)} %get-tuple-element.24), channel_id=1, source_target_pairs={{0,3},{1,2},{2,1},{3,0},{4,7},{5,6},{6,5},{7,4},{8,11},{9,10},{10,... | collective-permute-start | bytes 417800 | tf_op jit(solution)/shard_map/ppermute | solution.py:95
  33.9 13.7 %collective-permute-start.15 = (bf16[128,512]{1,0:T(8,128)(2,1)S(1)}, bf16[128,512]{1,0:T(8,128)(2,1)S(1)}, u32[]{:S(2)}, u32[]{:S(2)}) collective-permute-start(bf16[128,512]{1,0:T(8,128)(2,1)S(1)} %get-tuple-element.27), channel_id=1, source_target_pairs={{0,24},{1,25},{2,26},{3,27},{4,28},{5,29},{6,30},{7,31},{8,16},{9,... | collective-permute-start | bytes 393224 | tf_op jit(solution)/shard_map/ppermute | solution.py:95
  39.5 10.2 %collective-permute-start.4 = (bf16[136,512]{1,0:T(8,128)(2,1)S(1)}, bf16[136,512]{1,0:T(8,128)(2,1)S(1)}, u32[]{:S(2)}, u32[]{:S(2)}) collective-permute-start(bf16[136,512]{1,0:T(8,128)(2,1)S(1)} %shard_map.197.a), channel_id=1, source_target_pairs={{0,8},{1,9},{2,10},{3,11},{4,12},{5,13},{6,14},{7,15},{8,0},{9,1},... | collective-permute-start | bytes 417800 | tf_op jit(solution)/shard_map/ppermute | solution.py:95
  47.6 3.7 %collective-permute-start.20 = (bf16[128,512]{1,0:T(8,128)(2,1)S(1)}, bf16[128,512]{1,0:T(8,128)(2,1)S(1)}, u32[]{:S(2)}, u32[]{:S(2)}) collective-permute-start(bf16[128,512]{1,0:T(8,128)(2,1)S(1)} %collective-permute-done.15.refs_23_), channel_id=1, source_target_pairs={{0,4},{1,5},{2,6},{3,7},{4,0},{5,1},{6,2},{7,3},{8,12},{9,13},{10,... | collective-permute-start | bytes 393224 | tf_op jit(solution)/shard_map/ppermute | solution.py:95
  50.2 9.6 %collective-permute-start.5 = (bf16[136,512]{1,0:T(8,128)(2,1)S(1)}, bf16[136,512]{1,0:T(8,128)(2,1)S(1)}, u32[]{:S(2)}, u32[]{:S(2)}) collective-permute-start(bf16[136,512]{1,0:T(8,128)(2,1)S(1)} %shard_map.198.a), channel_id=1, source_target_pairs={{0,16},{1,17},{2,18},{3,19},{4,20},{5,21},{6,22},{7,23},{8,24},{9,... | collective-permute-start | bytes 417800 | tf_op jit(solution)/shard_map/ppermute | solution.py:95
  50.8 14.9 %collective-permute-start.10 = (bf16[576,512]{1,0:T(8,128)(2,1)S(1)}, bf16[576,512]{1,0:T(8,128)(2,1)S(1)}, u32[]{:S(2)}, u32[]{:S(2)}) collective-permute-start(bf16[576,512]{1,0:T(8,128)(2,1)S(1)} %get-tuple-element.25.refs_14_), channel_id=1, source_target_pairs={{0,4},{1,5},{2,6},{3,7},{4,0},{5,1},{6,2},{7,3},{8,12},{9,13},{10,... | collective-permute-start | bytes 1769480 | tf_op jit(solution)/shard_map/ppermute | solution.py:95
  50.8 16.0 %collective-permute-start.12 = (bf16[576,512]{1,0:T(8,128)(2,1)S(1)}, bf16[576,512]{1,0:T(8,128)(2,1)S(1)}, u32[]{:S(2)}, u32[]{:S(2)}) collective-permute-start(bf16[576,512]{1,0:T(8,128)(2,1)S(1)} %collective-permute-done.11.refs_16_), channel_id=1, source_target_pairs={{0,4},{1,5},{2,6},{3,7},{4,0},{5,1},{6,2},{7,3},{8,12},{9,13},{10,... | collective-permute-start | bytes 1769480 | tf_op jit(solution)/shard_map/ppermute | solution.py:95
  51.3 8.7 %collective-permute-start.16 = (bf16[128,512]{1,0:T(8,128)(2,1)S(1)}, bf16[128,512]{1,0:T(8,128)(2,1)S(1)}, u32[]{:S(2)}, u32[]{:S(2)}) collective-permute-start(bf16[128,512]{1,0:T(8,128)(2,1)S(1)} %collective-permute-done.15.refs_23_), channel_id=1, source_target_pairs={{0,8},{1,9},{2,10},{3,11},{4,12},{5,13},{6,14},{7,15},{8,0},{9,1},... | collective-permute-start | bytes 393224 | tf_op jit(solution)/shard_map/ppermute | solution.py:95
  53.1 13.2 %collective-permute-start.19 = (bf16[448,512]{1,0:T(8,128)(2,1)S(1)}, bf16[448,512]{1,0:T(8,128)(2,1)S(1)}, u32[]{:S(2)}, u32[]{:S(2)}) collective-permute-start(bf16[448,512]{1,0:T(8,128)(2,1)S(1)} %collective-permute-done.13.refs_22_), channel_id=1, source_target_pairs={{0,4},{1,5},{2,6},{3,7},{4,0},{5,1},{6,2},{7,3},{8,12},{9,13},{10,... | collective-permute-start | bytes 1376264 | tf_op jit(solution)/shard_map/ppermute | solution.py:95
  59.8 7.0 %collective-permute-start.17 = (bf16[448,512]{1,0:T(8,128)(2,1)S(1)}, bf16[448,512]{1,0:T(8,128)(2,1)S(1)}, u32[]{:S(2)}, u32[]{:S(2)}) collective-permute-start(bf16[448,512]{1,0:T(8,128)(2,1)S(1)} %collective-permute-done.14.refs_18_), channel_id=1, source_target_pairs={{0,4},{1,5},{2,6},{3,7},{4,0},{5,1},{6,2},{7,3},{8,12},{9,13},{10,... | collective-permute-start | bytes 1376264 | tf_op jit(solution)/shard_map/ppermute | solution.py:95
  60.0 1.9 %collective-permute-start.6 = (f32[128,512]{1,0:T(8,128)S(1)}, f32[128,512]{1,0:T(8,128)S(1)}, u32[]{:S(2)}, u32[]{:S(2)}) collective-permute-start(f32[128,512]{1,0:T(8,128)S(1)} %shard_map.199.a.refs_0_), channel_id=1, source_target_pairs={{0,4},{1,5},{2,6},{3,7},{4,0},{5,1},{6,2},{7,3},{8,12},{9,13},{10,... | collective-permute-start | bytes 786440 | tf_op jit(solution)/shard_map/ppermute | solution.py:95
  62.0 1.3 %collective-permute-start.18 = (bf16[128,512]{1,0:T(8,128)(2,1)S(1)}, bf16[128,512]{1,0:T(8,128)(2,1)S(1)}, u32[]{:S(2)}, u32[]{:S(2)}) collective-permute-start(bf16[128,512]{1,0:T(8,128)(2,1)S(1)} %collective-permute-done.16.refs_19_), channel_id=1, source_target_pairs={{0,4},{1,5},{2,6},{3,7},{4,0},{5,1},{6,2},{7,3},{8,12},{9,13},{10,... | collective-permute-start | bytes 393224 | tf_op jit(solution)/shard_map/ppermute | solution.py:95
  63.3 4.5 %collective-permute-start.9 = (f32[8,128]{1,0:T(8,128)S(1)}, f32[8,128]{1,0:T(8,128)S(1)}, u32[]{:S(2)}, u32[]{:S(2)}) collective-permute-start(f32[8,128]{1,0:T(8,128)S(1)} %shard_map.200.refs_2_), channel_id=1, source_target_pairs={{0,3},{1,2},{2,1},{3,0},{4,7},{5,6},{6,5},{7,4},{8,11},{9,10},{10,... | collective-permute-start | bytes 12296 | tf_op jit(solution)/shard_map/ppermute | solution.py:95
  65.8 3.6 %collective-permute-start.8 = (f32[8,128]{1,0:T(8,128)S(1)}, f32[8,128]{1,0:T(8,128)S(1)}, u32[]{:S(2)}, u32[]{:S(2)}) collective-permute-start(f32[8,128]{1,0:T(8,128)S(1)} %shard_map.200.refs_2_), channel_id=1, source_target_pairs={{0,2},{1,3},{2,0},{3,1},{4,6},{5,7},{6,4},{7,5},{8,10},{9,11},{10,... | collective-permute-start | bytes 12296 | tf_op jit(solution)/shard_map/ppermute | solution.py:95
  66.3 3.6 %collective-permute-start.7 = (f32[8,128]{1,0:T(8,128)S(1)}, f32[8,128]{1,0:T(8,128)S(1)}, u32[]{:S(2)}, u32[]{:S(2)}) collective-permute-start(f32[8,128]{1,0:T(8,128)S(1)} %shard_map.200.refs_2_), channel_id=1, source_target_pairs={{0,1},{1,0},{2,3},{3,2},{4,5},{5,4},{6,7},{7,6},{8,9},{9,8},{10,11... | collective-permute-start | bytes 12296 | tf_op jit(solution)/shard_map/ppermute | solution.py:95
  (5 other events, 298.2 us)

commit v3 on v2

--- a/solution.py
+++ b/solution.py
@@ -99,8 +99,8 @@
 VMEM = pl.BlockSpec(memory_space=pltpu.VMEM)
 HBM = pl.BlockSpec(memory_space=pltpu.HBM)
 TAG = 8
-PIECES = 2
-CUTS = (3,)
+PIECES = 4
+CUTS = (5,)
 
 
 def shape(*dims, dtype=jnp.float32):
@@ -263,24 +263,28 @@
 
 
 def pair_sum(a, b, last):
-    def kernel(a, b, out):
+    def kernel(a, b, out, *rest):
         value = get_coded(a) + get_coded(b)
         if last:
             out[...] = value
+            rest[0][...] = jnp.full(rest[0].shape, jnp.sum(value * value), jnp.float32)
         else:
             put_coded(out, value, unit_for(jnp.max(jnp.abs(value))))
 
     rows, cols = a.shape
-    out = shape(rows - TAG, cols) if last else shape(rows, cols, dtype=a.dtype)
-    return call(kernel, [out], (a, b), 8)[0]
-
-
-def square_sum(a, b):
-    def kernel(a, b, out):
-        value = jnp.sum(a[...] * a[...]) + jnp.sum(b[...] * b[...])
-        out[...] = jnp.full(out.shape, value, jnp.float32)
-
-    return call(kernel, [shape(8, 128)], (a, b), 4)[0]
+    if last:
+        return call(kernel, [shape(rows - TAG, cols), shape(8, 128)], (a, b), 8)
+    return call(kernel, [shape(rows, cols, dtype=a.dtype)], (a, b), 8)[0]
+
+
+def add_squares(parts):
+    def kernel(*refs):
+        value = refs[0][...]
+        for ref in refs[1:-1]:
+            value = value + ref[...]
+        refs[-1][...] = value
+
+    return call(kernel, [shape(*parts[0].shape)], parts, 4)[0]
 
 
 def finish(entries, total, other, squares, bases, masters, old, blocks):
@@ -288,8 +292,16 @@
     full, rank = bases[0].shape
     here = old[0].shape[0]
     n_sq, n_bl = len(squares), len(blocks)
-    piece = rows // PIECES
     flat = [a for block in blocks for a in block]
+
+    def spans(n, row, size):
+        found, edge = [], 0
+        for a in blocks[n]:
+            first, last = max(edge, row), min(edge + a.shape[0], row + size)
+            if first < last:
+                found.append((first - row, last - first))
+            edge += a.shape[0]
+        return found
 
     def kernel(*refs):
         refs = list(refs)
@@ -341,21 +353,20 @@
                     value - high.astype(jnp.float32)
                 ).astype(jnp.bfloat16)
             for n in range(n_bl):
-                for p in range(PIECES):
-                    row0 = pl.multiple_of((me ^ n) * rows + p * piece, piece)
-                    b = basis_refs[which][pl.ds(row0, piece), :]
-                    both = jnp.concatenate([b, b], axis=1)
-                    down = jnp.dot(both, direction[which], preferred_element_type=jnp.float32)
-                    at = slice(p * piece, (p + 1) * piece)
-                    if n == 0:
-                        own[which, at, :] = -down
-                        own[2 + which, at, :] = master_refs[which][at, :] - down
-                    value = packed(n, 4 * here + which * rows + p * piece, piece)
-                    stage[2 * n + which, at, :] = (value - down).astype(jnp.bfloat16)
+                row0 = pl.multiple_of((me ^ n) * rows, rows)
+                b = basis_refs[which][pl.ds(row0, rows), :]
+                both = jnp.concatenate([b, b], axis=1)
+                down = jnp.dot(both, direction[which], preferred_element_type=jnp.float32)
+                if n == 0:
+                    own[which] = -down
+                    own[2 + which] = master_refs[which][...] - down
+                for first, size in spans(n, 4 * here + which * rows, rows):
+                    value = packed(n, 4 * here + which * rows + first, size)
+                    at = slice(first, first + size)
+                    stage[2 * n + which, at, :] = (value - down[at, :]).astype(jnp.bfloat16)
                 if n == 0:
                     for j in (which, 2 + which):
                         send(own.at[j], outs[4 + j])
-                row0 = pl.multiple_of((me ^ n) * rows, rows)
                 send(stage.at[2 * n + which], outs[8 + which].at[pl.ds(row0, rows), :])
         for which in range(2):
             grad = grads[which, pl.ds(pl.multiple_of(me * here, here), here), :]
@@ -415,13 +426,13 @@
     got = [exchange(coded[k - 1], 0, k) for k in range(1, tp_count)]
     coded = plane_sum(mine, got)
     coded = pair_sum(coded, exchange(coded, CORES), False)
-    total = pair_sum(coded, exchange(coded, 2 * CORES), True)
+    total, squares = pair_sum(coded, exchange(coded, 2 * CORES), True)
     two = [exchange(t, CORES) for t in three]
 
     other = exchange(total, 1)
-    squares = square_sum(total, other)
-    squares = [squares] + [exchange(squares, 0, k) for k in range(1, tp_count)]
-
+    got = [exchange(squares, 0, k) for k in range(1, tp_count)]
+    squares = add_squares((squares, *got))
+    squares = (squares, exchange(squares, 1))
     blocks = [[whole], [exchange(whole, 1)], [one], [exchange(one, 1)]]
     for arrays in (two, three):
         blocks += [arrays, [exchange(a, 1) for a in arrays]]

time: 75.2 us -> 84.1 us (1.12)
  waiting for transfers between devices: 34 us -> 52.1 us
  starting transfers between devices: 28.8 us -> 19.7 us
    ppermute x21 -> x22, waiting for transfers between devices: 34 us -> 52.1 us  [exchange(): return lax.ppermute(x, ('fs', 'tp'), pairs)]
    ppermute x21 -> x22, starting transfers between devices: 28.8 us -> 19.7 us  [exchange(): return lax.ppermute(x, ('fs', 'tp'), pairs)]
  transfers between devices with their start and end apart: 21 -> 22, of which waited for: 10 -> 9; matrix products, arithmetic and copies ran while one was open for 0% -> 0% of each run, Pallas kernels for 5% -> 4%
where the time goes in v3:
time: 84.1 us; the launch traced here: 84 us
  waiting for transfers between devices  52.1 us (62%)
  starting transfers between devices  19.7 us (23%)
  Pallas kernels  11.3 us (13%)
  between operations  0.85 us (1%)
    ppermute x22, waiting for transfers between devices, exchange(): return lax.ppermute(x, ('fs', 'tp'), pairs)  52.1 us
    ppermute x22, starting transfers between devices, exchange(): return lax.ppermute(x, ('fs', 'tp'), pairs)  19.7 us
    pallas_call x8, Pallas kernels, call(): pl.pallas_call(kernel, out_shape=outs, in_specs=[HBM if hbm_args else VME...  11.3 us
  transfers between devices with their start and end apart: 22, of which 9 were waited for; matrix products, arithmetic and copies ran while one was open for 0% of the time, Pallas kernels for 4%

profile of v3, /device:TPU:0, one launch (start us, length us, event | category | flops | bytes accessed | tf_op | source)
XLA Modules:
  0.0 84.0 jit_solution(14219949977837343268)
XLA Ops:
  0.6 2.9 %shard_map.195 = (f32[128,2048]{1,0:T(8,128)S(1)}, f32[128,2048]{1,0:T(8,128)S(1)}) custom-call(bf16[2048,128]{1,0:T(8,128)(2,1)} %refs_4_.5, bf16[192,2048]{1,0:T(8,128)(2,1)} %refs_1_.2, bf16[2048,128]{1,0:T(8,128)(2,1)} %refs_5_.5, bf16[192,2048]{1,0:T(8,128)(2,1)} %refs_3_.2, bf16[192,2048]{1,0:T(8,128)(2,1)} %refs_4_.3, bf16[192,2048]{1,0:T(8,128)(2,1)} %refs_5_.3), custom_call_target="tpu_custom_call" | custom-call | tf_op jit(solution)/shard_map/pallas_call | solution.py:129
  3.5 0.6 collective-permute-start
  4.1 1.5 %shard_map.201 = (bf16[576,512]{1,0:T(8,128)(2,1)S(1)}, bf16[384,512]{1,0:T(8,128)(2,1)S(1)}, bf16[192,512]{1,0:T(8,128)(2,1)S(1)}) custom-call(f32[16,512]{1,0:T(8,128)} %refs_8_.1, f32[16,512]{1,0:T(8,128)} %refs_9_.1, f32[16,512]{1,0:T(8,128)} %refs_10_.1, f32[16,512]{1,0:T(8,128)} %refs_11_.1, f32[256,512]{1,0:T(8,128)} %refs_6_.1, f32[256,512]{1,0:T(8,128)} %refs_7_.1), custom_call_target="tpu_custom_call" | custom-call | tf_op jit(solution)/shard_map/pallas_call | solution.py:129
  5.6 2.7 %collective-permute-start.12 = (bf16[576,512]{1,0:T(8,128)(2,1)S(1)}, bf16[576,512]{1,0:T(8,128)(2,1)S(1)}, u32[]{:S(2)}, u32[]{:S(2)}) collective-permute-start(bf16[576,512]{1,0:T(8,128)(2,1)S(1)} %get-tuple-element.29.refs_12_), channel_id=1, source_target_pairs={{0,8},{1,9},{2,10},{3,11},{4,12},{5,13},{6,14},{7,15},{8,0},{9,1},... | collective-permute-start | bytes 1769480 | tf_op jit(solution)/shard_map/ppermute | solution.py:95
  8.3 2.5 %collective-permute-start.14 = (bf16[384,512]{1,0:T(8,128)(2,1)S(1)}, bf16[384,512]{1,0:T(8,128)(2,1)S(1)}, u32[]{:S(2)}, u32[]{:S(2)}) collective-permute-start(bf16[384,512]{1,0:T(8,128)(2,1)S(1)} %get-tuple-element.30), channel_id=1, source_target_pairs={{0,24},{1,25},{2,26},{3,27},{4,28},{5,29},{6,30},{7,31},{8,16},{9,... | collective-permute-start | bytes 1179656 | tf_op jit(solution)/shard_map/ppermute | solution.py:95
  10.7 1.4 %collective-permute-start.16 = (bf16[192,512]{1,0:T(8,128)(2,1)S(1)}, bf16[192,512]{1,0:T(8,128)(2,1)S(1)}, u32[]{:S(2)}, u32[]{:S(2)}) collective-permute-start(bf16[192,512]{1,0:T(8,128)(2,1)S(1)} %get-tuple-element.31), channel_id=1, source_target_pairs={{0,24},{1,25},{2,26},{3,27},{4,28},{5,29},{6,30},{7,31},{8,16},{9,... | collective-permute-start | bytes 589832 | tf_op jit(solution)/shard_map/ppermute | solution.py:95
  12.1 0.6 shard_map.196
  12.7 1.6 %collective-permute-start.1 = (bf16[136,512]{1,0:T(8,128)(2,1)S(1)}, bf16[136,512]{1,0:T(8,128)(2,1)S(1)}, u32[]{:S(2)}, u32[]{:S(2)}) collective-permute-start(bf16[136,512]{1,0:T(8,128)(2,1)S(1)} %get-tuple-element.24), channel_id=1, source_target_pairs={{0,1},{1,0},{2,3},{3,2},{4,5},{5,4},{6,7},{7,6},{8,9},{9,8},{10,11... | collective-permute-start | bytes 417800 | tf_op jit(solution)/shard_map/ppermute | solution.py:95
  14.3 1.5 %collective-permute-start.2 = (bf16[136,512]{1,0:T(8,128)(2,1)S(1)}, bf16[136,512]{1,0:T(8,128)(2,1)S(1)}, u32[]{:S(2)}, u32[]{:S(2)}) collective-permute-start(bf16[136,512]{1,0:T(8,128)(2,1)S(1)} %get-tuple-element.25), channel_id=1, source_target_pairs={{0,2},{1,3},{2,0},{3,1},{4,6},{5,7},{6,4},{7,5},{8,10},{9,11},{10,... | collective-permute-start | bytes 417800 | tf_op jit(solution)/shard_map/ppermute | solution.py:95
  15.8 21.4 %collective-permute-done.16.refs_21_ = bf16[192,512]{1,0:T(8,128)(2,1)S(1)} collective-permute-done((bf16[192,512]{1,0:T(8,128)(2,1)S(1)}, bf16[192,512]{1,0:T(8,128)(2,1)S(1)}, u32[]{:S(2)}, u32[]{:S(2)}) %collective-permute-start.16) | collective-permute-done | bytes 196640 | tf_op jit(solution)/shard_map/ppermute | solution.py:95
  37.2 2.5 %collective-permute-start.3 = (bf16[136,512]{1,0:T(8,128)(2,1)S(1)}, bf16[136,512]{1,0:T(8,128)(2,1)S(1)}, u32[]{:S(2)}, u32[]{:S(2)}) collective-permute-start(bf16[136,512]{1,0:T(8,128)(2,1)S(1)} %get-tuple-element.26), channel_id=1, source_target_pairs={{0,3},{1,2},{2,1},{3,0},{4,7},{5,6},{6,5},{7,4},{8,11},{9,10},{10,... | collective-permute-start | bytes 417800 | tf_op jit(solution)/shard_map/ppermute | solution.py:95
  39.7 0.6 collective-permute-start.15
  40.2 3.0 %collective-permute-done.3.refs_2_ = bf16[136,512]{1,0:T(8,128)(2,1)S(1)} collective-permute-done((bf16[136,512]{1,0:T(8,128)(2,1)S(1)}, bf16[136,512]{1,0:T(8,128)(2,1)S(1)}, u32[]{:S(2)}, u32[]{:S(2)}) %collective-permute-start.3) | collective-permute-done | bytes 139296 | tf_op jit(solution)/shard_map/ppermute | solution.py:95
  43.8 0.5 collective-permute-start.4
  44.3 1.5 %collective-permute-start.17 = (bf16[192,512]{1,0:T(8,128)(2,1)S(1)}, bf16[192,512]{1,0:T(8,128)(2,1)S(1)}, u32[]{:S(2)}, u32[]{:S(2)}) collective-permute-start(bf16[192,512]{1,0:T(8,128)(2,1)S(1)} %collective-permute-done.16.refs_21_), channel_id=1, source_target_pairs={{0,8},{1,9},{2,10},{3,11},{4,12},{5,13},{6,14},{7,15},{8,0},{9,1},... | collective-permute-start | bytes 589832 | tf_op jit(solution)/shard_map/ppermute | solution.py:95
  45.9 8.7 %collective-permute-done.4.b = bf16[136,512]{1,0:T(8,128)(2,1)S(1)} collective-permute-done((bf16[136,512]{1,0:T(8,128)(2,1)S(1)}, bf16[136,512]{1,0:T(8,128)(2,1)S(1)}, u32[]{:S(2)}, u32[]{:S(2)}) %collective-permute-start.4) | collective-permute-done | bytes 139296 | tf_op jit(solution)/shard_map/ppermute | solution.py:95
  55.1 1.8 %collective-permute-start.5 = (bf16[136,512]{1,0:T(8,128)(2,1)S(1)}, bf16[136,512]{1,0:T(8,128)(2,1)S(1)}, u32[]{:S(2)}, u32[]{:S(2)}) collective-permute-start(bf16[136,512]{1,0:T(8,128)(2,1)S(1)} %shard_map.198.a), channel_id=1, source_target_pairs={{0,16},{1,17},{2,18},{3,19},{4,20},{5,21},{6,22},{7,23},{8,24},{9,... | collective-permute-start | bytes 417800 | tf_op jit(solution)/shard_map/ppermute | solution.py:95
  57.7 7.4 %collective-permute-done.5.b = bf16[136,512]{1,0:T(8,128)(2,1)S(1)} collective-permute-done((bf16[136,512]{1,0:T(8,128)(2,1)S(1)}, bf16[136,512]{1,0:T(8,128)(2,1)S(1)}, u32[]{:S(2)}, u32[]{:S(2)}) %collective-permute-start.5) | collective-permute-done | bytes 139296 | tf_op jit(solution)/shard_map/ppermute | solution.py:95
  66.1 4.0 %collective-permute-done.9.refs_3_ = f32[8,128]{1,0:T(8,128)S(1)} collective-permute-done((f32[8,128]{1,0:T(8,128)S(1)}, f32[8,128]{1,0:T(8,128)S(1)}, u32[]{:S(2)}, u32[]{:S(2)}) %collective-permute-start.9) | collective-permute-done | bytes 4128 | tf_op jit(solution)/shard_map/ppermute | solution.py:95
  70.6 3.1 %collective-permute-done.8.refs_2_ = f32[8,128]{1,0:T(8,128)S(1)} collective-permute-done((f32[8,128]{1,0:T(8,128)S(1)}, f32[8,128]{1,0:T(8,128)S(1)}, u32[]{:S(2)}, u32[]{:S(2)}) %collective-permute-start.8) | collective-permute-done | bytes 4128 | tf_op jit(solution)/shard_map/ppermute | solution.py:95
  74.2 3.1 %collective-permute-done.7.refs_1_ = f32[8,128]{1,0:T(8,128)S(1)} collective-permute-done((f32[8,128]{1,0:T(8,128)S(1)}, f32[8,128]{1,0:T(8,128)S(1)}, u32[]{:S(2)}, u32[]{:S(2)}) %collective-permute-start.7) | collective-permute-done | bytes 4128 | tf_op jit(solution)/shard_map/ppermute | solution.py:95
  77.4 0.6 collective-permute-start.10
  77.9 0.9 %collective-permute-done.10.refs_3_ = f32[8,128]{1,0:T(8,128)S(1)} collective-permute-done((f32[8,128]{1,0:T(8,128)S(1)}, f32[8,128]{1,0:T(8,128)S(1)}, u32[]{:S(2)}, u32[]{:S(2)}) %collective-permute-start.10) | collective-permute-done | bytes 4128 | tf_op jit(solution)/shard_map/ppermute | solution.py:95
  78.9 5.0 %shard_map.202 = (f32[16,512]{1,0:T(8,128)}, f32[16,512]{1,0:T(8,128)}, f32[16,512]{1,0:T(8,128)}, f32[16,512]{1,0:T(8,128)}, f32[256,512]{1,0:T(8,128)}, /*inde...) custom-call(f32[128,512]{1,0:T(8,128)S(1)} %get-tuple-element.27.ref, ...), custom_call_target="tpu_custom_call" | custom-call | tf_op jit(solution)/shard_map/pallas_call | solution.py:129
  (44 shorter events, 3.8 us)
Async XLA Ops:
  3.5 8.6 %collective-permute-start = (f32[128,2048]{1,0:T(8,128)S(1)}, f32[128,2048]{1,0:T(8,128)S(1)}, u32[]{:S(2)}, u32[]{:S(2)}) collective-permute-start(f32[128,2048]{1,0:T(8,128)S(1)} %get-tuple-element.22), channel_id=1, source_target_pairs={{0,4},{1,5},{2,6},{3,7},{4,0},{5,1},{6,2},{7,3},{8,12},{9,13},{10,... | collective-permute-start | bytes 3145736 | tf_op jit(solution)/shard_map/ppermute | solution.py:95
  5.5 73.3 %copy-start = (f32[256,512]{1,0:T(8,128)S(1)}, f32[256,512]{1,0:T(8,128)}, u32[]{:S(2)}) copy-start(f32[256,512]{1,0:T(8,128)} %refs_6_.1) | copy-start | bytes 1572868
  5.5 73.3 %copy-start.1 = (f32[256,512]{1,0:T(8,128)S(1)}, f32[256,512]{1,0:T(8,128)}, u32[]{:S(2)}) copy-start(f32[256,512]{1,0:T(8,128)} %refs_7_.1) | copy-start | bytes 1572868
  5.6 40.3 %collective-permute-start.12 = (bf16[576,512]{1,0:T(8,128)(2,1)S(1)}, bf16[576,512]{1,0:T(8,128)(2,1)S(1)}, u32[]{:S(2)}, u32[]{:S(2)}) collective-permute-start(bf16[576,512]{1,0:T(8,128)(2,1)S(1)} %get-tuple-element.29.refs_12_), channel_id=1, source_target_pairs={{0,8},{1,9},{2,10},{3,11},{4,12},{5,13},{6,14},{7,15},{8,0},{9,1},... | collective-permute-start | bytes 1769480 | tf_op jit(solution)/shard_map/ppermute | solution.py:95
  8.3 31.4 %collective-permute-start.14 = (bf16[384,512]{1,0:T(8,128)(2,1)S(1)}, bf16[384,512]{1,0:T(8,128)(2,1)S(1)}, u32[]{:S(2)}, u32[]{:S(2)}) collective-permute-start(bf16[384,512]{1,0:T(8,128)(2,1)S(1)} %get-tuple-element.30), channel_id=1, source_target_pairs={{0,24},{1,25},{2,26},{3,27},{4,28},{5,29},{6,30},{7,31},{8,16},{9,... | collective-permute-start | bytes 1179656 | tf_op jit(solution)/shard_map/ppermute | solution.py:95
  10.7 26.4 %collective-permute-start.16 = (bf16[192,512]{1,0:T(8,128)(2,1)S(1)}, bf16[192,512]{1,0:T(8,128)(2,1)S(1)}, u32[]{:S(2)}, u32[]{:S(2)}) collective-permute-start(bf16[192,512]{1,0:T(8,128)(2,1)S(1)} %get-tuple-element.31), channel_id=1, source_target_pairs={{0,24},{1,25},{2,26},{3,27},{4,28},{5,29},{6,30},{7,31},{8,16},{9,... | collective-permute-start | bytes 589832 | tf_op jit(solution)/shard_map/ppermute | solution.py:95
  12.7 27.5 %collective-permute-start.1 = (bf16[136,512]{1,0:T(8,128)(2,1)S(1)}, bf16[136,512]{1,0:T(8,128)(2,1)S(1)}, u32[]{:S(2)}, u32[]{:S(2)}) collective-permute-start(bf16[136,512]{1,0:T(8,128)(2,1)S(1)} %get-tuple-element.24), channel_id=1, source_target_pairs={{0,1},{1,0},{2,3},{3,2},{4,5},{5,4},{6,7},{7,6},{8,9},{9,8},{10,11... | collective-permute-start | bytes 417800 | tf_op jit(solution)/shard_map/ppermute | solution.py:95
  14.3 26.0 %collective-permute-start.2 = (bf16[136,512]{1,0:T(8,128)(2,1)S(1)}, bf16[136,512]{1,0:T(8,128)(2,1)S(1)}, u32[]{:S(2)}, u32[]{:S(2)}) collective-permute-start(bf16[136,512]{1,0:T(8,128)(2,1)S(1)} %get-tuple-element.25), channel_id=1, source_target_pairs={{0,2},{1,3},{2,0},{3,1},{4,6},{5,7},{6,4},{7,5},{8,10},{9,11},{10,... | collective-permute-start | bytes 417800 | tf_op jit(solution)/shard_map/ppermute | solution.py:95
  37.2 6.1 %collective-permute-start.3 = (bf16[136,512]{1,0:T(8,128)(2,1)S(1)}, bf16[136,512]{1,0:T(8,128)(2,1)S(1)}, u32[]{:S(2)}, u32[]{:S(2)}) collective-permute-start(bf16[136,512]{1,0:T(8,128)(2,1)S(1)} %get-tuple-element.26), channel_id=1, source_target_pairs={{0,3},{1,2},{2,1},{3,0},{4,7},{5,6},{6,5},{7,4},{8,11},{9,10},{10,... | collective-permute-start | bytes 417800 | tf_op jit(solution)/shard_map/ppermute | solution.py:95
  39.7 17.5 %collective-permute-start.15 = (bf16[384,512]{1,0:T(8,128)(2,1)S(1)}, bf16[384,512]{1,0:T(8,128)(2,1)S(1)}, u32[]{:S(2)}, u32[]{:S(2)}) collective-permute-start(bf16[384,512]{1,0:T(8,128)(2,1)S(1)} %collective-permute-done.14.refs_20_), channel_id=1, source_target_pairs={{0,8},{1,9},{2,10},{3,11},{4,12},{5,13},{6,14},{7,15},{8,0},{9,1},... | collective-permute-start | bytes 1179656 | tf_op jit(solution)/shard_map/ppermute | solution.py:95
  40.2 14.9 %collective-permute-start.21 = (bf16[192,512]{1,0:T(8,128)(2,1)S(1)}, bf16[192,512]{1,0:T(8,128)(2,1)S(1)}, u32[]{:S(2)}, u32[]{:S(2)}) collective-permute-start(bf16[192,512]{1,0:T(8,128)(2,1)S(1)} %collective-permute-done.16.refs_21_), channel_id=1, source_target_pairs={{0,4},{1,5},{2,6},{3,7},{4,0},{5,1},{6,2},{7,3},{8,12},{9,13},{10,... | collective-permute-start | bytes 589832 | tf_op jit(solution)/shard_map/ppermute | solution.py:95
  43.8 10.8 %collective-permute-start.4 = (bf16[136,512]{1,0:T(8,128)(2,1)S(1)}, bf16[136,512]{1,0:T(8,128)(2,1)S(1)}, u32[]{:S(2)}, u32[]{:S(2)}) collective-permute-start(bf16[136,512]{1,0:T(8,128)(2,1)S(1)} %shard_map.197.a), channel_id=1, source_target_pairs={{0,8},{1,9},{2,10},{3,11},{4,12},{5,13},{6,14},{7,15},{8,0},{9,1},... | collective-permute-start | bytes 417800 | tf_op jit(solution)/shard_map/ppermute | solution.py:95
  44.3 12.8 %collective-permute-start.17 = (bf16[192,512]{1,0:T(8,128)(2,1)S(1)}, bf16[192,512]{1,0:T(8,128)(2,1)S(1)}, u32[]{:S(2)}, u32[]{:S(2)}) collective-permute-start(bf16[192,512]{1,0:T(8,128)(2,1)S(1)} %collective-permute-done.16.refs_21_), channel_id=1, source_target_pairs={{0,8},{1,9},{2,10},{3,11},{4,12},{5,13},{6,14},{7,15},{8,0},{9,1},... | collective-permute-start | bytes 589832 | tf_op jit(solution)/shard_map/ppermute | solution.py:95
  45.9 31.5 %collective-permute-start.11 = (bf16[576,512]{1,0:T(8,128)(2,1)S(1)}, bf16[576,512]{1,0:T(8,128)(2,1)S(1)}, u32[]{:S(2)}, u32[]{:S(2)}) collective-permute-start(bf16[576,512]{1,0:T(8,128)(2,1)S(1)} %get-tuple-element.29.refs_12_), channel_id=1, source_target_pairs={{0,4},{1,5},{2,6},{3,7},{4,0},{5,1},{6,2},{7,3},{8,12},{9,13},{10,... | collective-permute-start | bytes 1769480 | tf_op jit(solution)/shard_map/ppermute | solution.py:95
  54.6 23.3 %collective-permute-start.13 = (bf16[576,512]{1,0:T(8,128)(2,1)S(1)}, bf16[576,512]{1,0:T(8,128)(2,1)S(1)}, u32[]{:S(2)}, u32[]{:S(2)}) collective-permute-start(bf16[576,512]{1,0:T(8,128)(2,1)S(1)} %collective-permute-done.12.refs_14_), channel_id=1, source_target_pairs={{0,4},{1,5},{2,6},{3,7},{4,0},{5,1},{6,2},{7,3},{8,12},{9,13},{10,... | collective-permute-start | bytes 1769480 | tf_op jit(solution)/shard_map/ppermute | solution.py:95
  55.1 10.0 %collective-permute-start.5 = (bf16[136,512]{1,0:T(8,128)(2,1)S(1)}, bf16[136,512]{1,0:T(8,128)(2,1)S(1)}, u32[]{:S(2)}, u32[]{:S(2)}) collective-permute-start(bf16[136,512]{1,0:T(8,128)(2,1)S(1)} %shard_map.198.a), channel_id=1, source_target_pairs={{0,16},{1,17},{2,18},{3,19},{4,20},{5,21},{6,22},{7,23},{8,24},{9,... | collective-permute-start | bytes 417800 | tf_op jit(solution)/shard_map/ppermute | solution.py:95
  57.2 8.4 %collective-permute-start.19 = (bf16[192,512]{1,0:T(8,128)(2,1)S(1)}, bf16[192,512]{1,0:T(8,128)(2,1)S(1)}, u32[]{:S(2)}, u32[]{:S(2)}) collective-permute-start(bf16[192,512]{1,0:T(8,128)(2,1)S(1)} %collective-permute-done.17.refs_17_), channel_id=1, source_target_pairs={{0,4},{1,5},{2,6},{3,7},{4,0},{5,1},{6,2},{7,3},{8,12},{9,13},{10,... | collective-permute-start | bytes 589832 | tf_op jit(solution)/shard_map/ppermute | solution.py:95
  57.2 20.7 %collective-permute-start.20 = (bf16[384,512]{1,0:T(8,128)(2,1)S(1)}, bf16[384,512]{1,0:T(8,128)(2,1)S(1)}, u32[]{:S(2)}, u32[]{:S(2)}) collective-permute-start(bf16[384,512]{1,0:T(8,128)(2,1)S(1)} %collective-permute-done.14.refs_20_), channel_id=1, source_target_pairs={{0,4},{1,5},{2,6},{3,7},{4,0},{5,1},{6,2},{7,3},{8,12},{9,13},{10,... | collective-permute-start | bytes 1179656 | tf_op jit(solution)/shard_map/ppermute | solution.py:95
  65.1 12.8 %collective-permute-start.18 = (bf16[384,512]{1,0:T(8,128)(2,1)S(1)}, bf16[384,512]{1,0:T(8,128)(2,1)S(1)}, u32[]{:S(2)}, u32[]{:S(2)}) collective-permute-start(bf16[384,512]{1,0:T(8,128)(2,1)S(1)} %collective-permute-done.15.refs_16_), channel_id=1, source_target_pairs={{0,4},{1,5},{2,6},{3,7},{4,0},{5,1},{6,2},{7,3},{8,12},{9,13},{10,... | collective-permute-start | bytes 1179656 | tf_op jit(solution)/shard_map/ppermute | solution.py:95
  65.5 4.6 %collective-permute-start.9 = (f32[8,128]{1,0:T(8,128)S(1)}, f32[8,128]{1,0:T(8,128)S(1)}, u32[]{:S(2)}, u32[]{:S(2)}) collective-permute-start(f32[8,128]{1,0:T(8,128)S(1)} %get-tuple-element.28.refs_0_), channel_id=1, source_target_pairs={{0,3},{1,2},{2,1},{3,0},{4,7},{5,6},{6,5},{7,4},{8,11},{9,10},{10,... | collective-permute-start | bytes 12296 | tf_op jit(solution)/shard_map/ppermute | solution.py:95
  70.1 3.6 %collective-permute-start.8 = (f32[8,128]{1,0:T(8,128)S(1)}, f32[8,128]{1,0:T(8,128)S(1)}, u32[]{:S(2)}, u32[]{:S(2)}) collective-permute-start(f32[8,128]{1,0:T(8,128)S(1)} %get-tuple-element.28.refs_0_), channel_id=1, source_target_pairs={{0,2},{1,3},{2,0},{3,1},{4,6},{5,7},{6,4},{7,5},{8,10},{9,11},{10,... | collective-permute-start | bytes 12296 | tf_op jit(solution)/shard_map/ppermute | solution.py:95
  73.7 3.6 %collective-permute-start.7 = (f32[8,128]{1,0:T(8,128)S(1)}, f32[8,128]{1,0:T(8,128)S(1)}, u32[]{:S(2)}, u32[]{:S(2)}) collective-permute-start(f32[8,128]{1,0:T(8,128)S(1)} %get-tuple-element.28.refs_0_), channel_id=1, source_target_pairs={{0,1},{1,0},{2,3},{3,2},{4,5},{5,4},{6,7},{7,6},{8,9},{9,8},{10,11... | collective-permute-start | bytes 12296 | tf_op jit(solution)/shard_map/ppermute | solution.py:95
  77.3 1.5 %collective-permute-start.6 = (f32[128,512]{1,0:T(8,128)S(1)}, f32[128,512]{1,0:T(8,128)S(1)}, u32[]{:S(2)}, u32[]{:S(2)}) collective-permute-start(f32[128,512]{1,0:T(8,128)S(1)} %get-tuple-element.27.refs_0_), channel_id=1, source_target_pairs={{0,4},{1,5},{2,6},{3,7},{4,0},{5,1},{6,2},{7,3},{8,12},{9,13},{10,... | collective-permute-start | bytes 786440 | tf_op jit(solution)/shard_map/ppermute | solution.py:95
  77.4 1.5 %collective-permute-start.10 = (f32[8,128]{1,0:T(8,128)S(1)}, f32[8,128]{1,0:T(8,128)S(1)}, u32[]{:S(2)}, u32[]{:S(2)}) collective-permute-start(f32[8,128]{1,0:T(8,128)S(1)} %shard_map.200.refs_2_), channel_id=1, source_target_pairs={{0,4},{1,5},{2,6},{3,7},{4,0},{5,1},{6,2},{7,3},{8,12},{9,13},{10,... | collective-permute-start | bytes 12296 | tf_op jit(solution)/shard_map/ppermute | solution.py:95
  (6 other events, 440.0 us)
